TPU v7x, 32 devices: a whole 2x2x4 slice. The times are simulated.
32 devices in a mesh: sp: 8 (over z, y), tp: 4 (over x, core).
Axes of the slice: x: 2, y: 2, z: 4, core: 2. Of those that a mesh axis runs over, the one named last changes fastest.
Arguments:
- tokens: bfloat16 [8192, 2048], P(('sp', 'tp')), may hold values from -6 to 6
- norm_gain: float32 [2048], replicated, may hold values from 0.1 to 1.9
- w_query: bfloat16 [2048, 2048], P(None, 'tp'), may hold values from -0.125 to 0.125
- w_forget: bfloat16 [2048, 2048], P(None, 'tp'), may hold values from -0.125 to 0.125
- w_value: bfloat16 [2048, 2048], P(None, 'tp'), may hold values from -0.125 to 0.125
- w_rgate: bfloat16 [2048, 2048], P(None, 'tp'), may hold values from -0.125 to 0.125
- w_glu_value: bfloat16 [2048, 2048], P(None, 'tp'), may hold values from -0.125 to 0.125
- w_glu_gate: bfloat16 [2048, 2048], P(None, 'tp'), may hold values from -0.125 to 0.125
- forget_gap: float32 [2048], P('tp'), may hold values from 6.1035156e-05 to 0.1
- decay_shift: float32 [8192, 16], P('sp', 'tp'), may hold values from -0.6 to 0, as said below
- head_gain: float32 [128], replicated, may hold values from 0.1 to 1.9
- conv_taps: float32 [31, 2048], P(None, 'tp'), may hold values from -12 to 12
- conv_gain: float32 [2048], P('tp'), may hold values from 0.1 to 1.9
- out_rec: bfloat16 [2048, 2048], P('tp'), may hold values from -0.09375 to 0.09375
- out_conv: bfloat16 [2048, 2048], P('tp'), may hold values from -0.09375 to 0.09375
Outputs:
- mixed: bfloat16 [8192, 2048], P(('sp', 'tp'))
Inputs may be any that keep to these rules, and one draw needn't show every extreme that they name: `decay_shift`: at most zero everywhere.
All inputs are finite; a program needn't handle non-finite values.
Results may differ from a plain program's by a relative error of at most 0.015.
Values may be sent and summed in bfloat16 or wider, within the bound.
A program may use at most 128 MiB of HBM per device.

v0:
```python
import functools

import jax
import jax.numpy as jnp
from jax import lax
from jax.experimental import pallas as pl
from jax.experimental.pallas import tpu as pltpu
from jax.sharding import PartitionSpec as P

CHUNK = 128
PAD = 16
PIECES = 2
REACH = 32
TILE = 64
LANES = 128
MESH = pl.DeviceIdType.MESH

norm_epsilon = 1e-05
head_epsilon = 1e-06


def dot(a, b, dims=((1,), (0,))):
    return lax.dot_general(a, b, (dims, ((), ())), preferred_element_type=jnp.float32)


def layer_norm(values, gain):
    widened = values.astype(jnp.float32)
    row_mean = jnp.mean(widened, axis=-1, keepdims=True)
    centred = widened - row_mean
    row_var = jnp.mean(centred * centred, axis=-1, keepdims=True)
    return centred * lax.rsqrt(row_var + norm_epsilon) * gain


def partners():
    me = lax.axis_index("tp")
    pair = me + 1 - 2 * lax.rem(me, 2)
    return pair, lax.rem(me + 2, 4), lax.rem(pair + 2, 4), me


def greet(*others):
    barrier = pltpu.get_barrier_semaphore()
    for other in others:
        pl.semaphore_signal(barrier, inc=1, device_id={"tp": other}, device_id_type=MESH)
    pl.semaphore_wait(barrier, len(others))


def project_kernel(
    tokens_ref, gain_ref, w0, w1, w2, w3, w4, w5, out_ref,
    held, normed, weight, out, weight_sem, send_sem, recv_sem, out_sem,
):
    fetched = [pltpu.make_async_copy(w, weight.at[i], weight_sem.at[i]) for i, w in enumerate((w0, w1, w2, w3, w4, w5))]
    for one in fetched:
        one.start()
    pair, cross, diag, me = partners()
    greet(pair, cross)
    block = tokens_ref.shape[0]
    piece = block // PIECES

    def copy(source, target, kind, p, device):
        return pltpu.make_async_remote_copy(
            src_ref=source, dst_ref=target, send_sem=send_sem.at[kind, p], recv_sem=recv_sem.at[kind, p],
            device_id={"tp": device}, device_id_type=MESH,
        )

    parts = [pl.ds(p * piece, piece) for p in range(PIECES)]
    crossing = [copy(tokens_ref.at[rows, :], held.at[1, rows, :], 0, p, cross) for p, rows in enumerate(parts)]
    nearby = [copy(tokens_ref.at[rows, :], held.at[0, rows, :], 1, p, pair) for p, rows in enumerate(parts)]
    handed = [copy(held.at[1, rows, :], held.at[2, rows, :], 2, p, pair) for p, rows in enumerate(parts)]
    for one in crossing + nearby:
        one.start()
    stores = []

    def project(values, owner, p):
        normed[...] = layer_norm(values, gain_ref[...]).astype(jnp.bfloat16)
        if not stores:
            for one in fetched:
                one.wait()
        rows = pl.ds(pl.multiple_of(owner * block + p * piece, piece), piece)

        def step(i, carry):
            out[i, rows, :] = dot(normed[...], weight[i]).astype(jnp.bfloat16)
            return carry

        lax.fori_loop(0, len(fetched), step, 0)
        store = pltpu.make_async_copy(out.at[:, rows, :], out_ref.at[:, rows, :], out_sem.at[len(stores)])
        store.start()
        stores.append(store)

    for p, rows in enumerate(parts):
        project(tokens_ref[rows, :], me, p)
    for p, rows in enumerate(parts):
        nearby[p].wait_recv()
        project(held[0, rows, :], pair, p)
    for p, rows in enumerate(parts):
        crossing[p].wait_recv()
        handed[p].start()
        project(held[1, rows, :], cross, p)
        handed[p].wait_recv()
        project(held[2, rows, :], diag, p)
    for one in crossing + nearby + handed:
        one.wait_send()
    for one in stores:
        one.wait()


def gather_project(tokens, norm_gain, weights):
    block, depth = tokens.shape
    columns = weights[0].shape[1]
    rows = block * lax.axis_size("tp")
    count = len(weights)
    return pl.pallas_call(
        project_kernel,
        in_specs=[pl.BlockSpec(memory_space=pltpu.VMEM)] * 2 + [pl.BlockSpec(memory_space=pl.ANY)] * count,
        out_specs=pl.BlockSpec(memory_space=pl.ANY),
        out_shape=jax.ShapeDtypeStruct((count, rows, columns), jnp.bfloat16),
        scratch_shapes=[
            pltpu.VMEM((3, block, depth), jnp.bfloat16),
            pltpu.VMEM((block // PIECES, depth), jnp.bfloat16),
            pltpu.VMEM((count, depth, columns), jnp.bfloat16),
            pltpu.VMEM((count, rows, columns), jnp.bfloat16),
            pltpu.SemaphoreType.DMA((count,)),
            pltpu.SemaphoreType.DMA((3, PIECES)),
            pltpu.SemaphoreType.DMA((3, PIECES)),
            pltpu.SemaphoreType.DMA((4 * PIECES,)),
        ],
        compiler_params=pltpu.CompilerParams(
            collective_id=0, has_side_effects=True, vmem_limit_bytes=60000 * 1024
        ),
    )(tokens, norm_gain[None], *weights)


def scan_kernel(
    head, q_ref, f_ref, v_ref, gap_ref, shift_ref, near_ref, far_ref, pack_ref, state, offset
):
    step = pl.program_id(0)
    rows, width = q_ref.shape

    @pl.when(step == 0)
    def _():
        state[...] = jnp.zeros_like(state)
        offset[...] = jnp.zeros_like(offset)

    row = lax.broadcasted_iota(jnp.int32, (rows, rows), 0)
    col = lax.broadcasted_iota(jnp.int32, (rows, rows), 1)
    causal = row >= col
    lower = jnp.where(causal, 1.0, 0.0).astype(jnp.bfloat16)
    for h in range(width // head):
        part = slice(h * head, (h + 1) * head)
        query = q_ref[:, part].astype(jnp.float32)
        query = query * jax.nn.sigmoid(query)
        key = gap_ref[:, part] * jax.nn.sigmoid(-f_ref[:, part].astype(jnp.float32))
        log = jnp.log1p(-key) + shift_ref[:, h : h + 1]
        value = v_ref[:, part]
        high = log.astype(jnp.bfloat16)
        low = (log - high.astype(jnp.float32)).astype(jnp.bfloat16)
        total = dot(lower, high) + dot(lower, low)
        closing = total[rows - 1 : rows, :]
        middle = total[rows // 2 - 1 : rows // 2, :]
        query_mid = (query * jnp.exp(total - middle)).astype(jnp.bfloat16)
        key_mid = (key * jnp.exp(middle - total)).astype(jnp.bfloat16)
        scores = jnp.where(causal, dot(query_mid, key_mid, ((1,), (1,))), 0.0)
        query_near = query * jnp.exp(total)
        held = state[h]
        near_ref[:, part] = dot(scores.astype(jnp.bfloat16), value) + dot(
            query_near.astype(jnp.bfloat16), held.astype(jnp.bfloat16), ((1,), (1,))
        )
        far_ref[:, part] = (query_near * jnp.exp(offset[:, part])).astype(jnp.bfloat16)
        key_end = (key * jnp.exp(closing - total)).astype(jnp.bfloat16)
        state[h] = held * jnp.exp(closing) + dot(value, key_end, ((0,), (0,)))
        offset[:, part] = offset[:, part] + closing

    @pl.when(step == pl.num_programs(0) - 1)
    def _():
        place = lax.broadcasted_iota(jnp.int32, (PAD, head), 0)
        for h in range(width // head):
            pack_ref[h, 0:head, :] = state[h].astype(jnp.bfloat16)
            log = offset[:, h * head : (h + 1) * head]
            high = log.astype(jnp.bfloat16).astype(jnp.float32)
            rest = log - high
            mid = rest.astype(jnp.bfloat16).astype(jnp.float32)
            low = rest - mid
            tail = jnp.where(place == 0, high, jnp.where(place == 1, mid, jnp.where(place == 2, low, 0.0)))
            pack_ref[h, head : head + PAD, :] = tail.astype(jnp.bfloat16)


def local_scan(projected, forget_gap, decay_shift, head):
    rows, width = projected.shape[1:]
    heads = width // head

    def of(which):
        return pl.BlockSpec((None, CHUNK, width), lambda i: (which, i, 0))

    by_row = pl.BlockSpec((CHUNK, width), lambda i: (i, 0))
    whole = lambda shape: pl.BlockSpec(shape, lambda i: (0,) * len(shape))
    return pl.pallas_call(
        functools.partial(scan_kernel, head),
        grid=(rows // CHUNK,),
        in_specs=[
            of(0),
            of(1),
            of(2),
            whole((1, width)),
            pl.BlockSpec((CHUNK, heads), lambda i: (i, 0)),
        ],
        out_specs=[by_row, by_row, whole((heads, head + PAD, head))],
        out_shape=[
            jax.ShapeDtypeStruct((rows, width), jnp.float32),
            jax.ShapeDtypeStruct((rows, width), jnp.bfloat16),
            jax.ShapeDtypeStruct((heads, head + PAD, head), jnp.bfloat16),
        ],
        scratch_shapes=[
            pltpu.VMEM((heads, head, head), jnp.float32),
            pltpu.VMEM((1, width), jnp.float32),
        ],
        compiler_params=pltpu.CompilerParams(dimension_semantics=("arbitrary",)),
        cost_estimate=pl.CostEstimate(
            flops=rows * width * head * 12, bytes_accessed=rows * width * 12, transcendentals=rows * width * 8
        ),
    )(projected, projected, projected, forget_gap[None], decay_shift)


def exchange_kernel(
    head, pack_ref, glu_value_ref, glu_gate_ref, taps_ref, arriving_ref, filtered_ref, stats_ref,
    gathered, rim, padded, own_stats, other_stats, send_sem, recv_sem, rim_sem, stat_send, stat_recv,
):
    me, tp = lax.axis_index("sp"), lax.axis_index("tp")
    count, groups = gathered.shape[0] + 1, other_stats.shape[0] + 1
    rows, width = filtered_ref.shape
    taps = taps_ref.shape[0]
    barrier = pltpu.get_barrier_semaphore()
    for k in range(1, count):
        pl.semaphore_signal(barrier, inc=1, device_id={"sp": lax.rem(me + k, count)}, device_id_type=MESH)
    for k in range(1, groups):
        pl.semaphore_signal(barrier, inc=1, device_id={"tp": lax.rem(tp + k, groups)}, device_id_type=MESH)
    pl.semaphore_wait(barrier, count + groups - 2)

    def mix(at, size):
        gate = glu_gate_ref[pl.ds(at, size), :].astype(jnp.float32)
        value = glu_value_ref[pl.ds(at, size), :].astype(jnp.float32)
        return (value * jax.nn.sigmoid(gate)).astype(jnp.bfloat16)

    after = lax.rem(me + 1, count)
    rim[0] = mix(rows - REACH, REACH)
    edge = pltpu.make_async_remote_copy(
        src_ref=rim.at[0], dst_ref=rim.at[1], send_sem=rim_sem.at[0], recv_sem=rim_sem.at[1],
        device_id={"sp": after}, device_id_type=MESH,
    )
    states = [
        pltpu.make_async_remote_copy(
            src_ref=pack_ref, dst_ref=gathered.at[k - 1], send_sem=send_sem.at[k - 1], recv_sem=recv_sem.at[k - 1],
            device_id={"sp": lax.rem(me + k, count)}, device_id_type=MESH,
        )
        for k in range(1, count)
    ]
    edge.start()
    for k, state in enumerate(states, 1):
        pl.when(me + k < count)(state.start)

    def mix_tile(i, carry):
        at = pl.multiple_of(i * TILE, TILE)
        padded[pl.ds(pl.multiple_of(at + REACH, 16), TILE), :] = mix(at, TILE).astype(jnp.float32)
        return carry

    lax.fori_loop(0, rows // TILE, mix_tile, 0)
    edge.wait_recv()
    padded[0:REACH, :] = jnp.where(me > 0, rim[1].astype(jnp.float32), 0.0)

    pick = lax.broadcasted_iota(jnp.int32, (8, LANES), 0)
    first = jnp.where(pick == 0, 1.0, 0.0)
    second = jnp.where(pick == 1, 1.0, 0.0)
    skip = REACH - taps + 1

    def filter_tile(i, carry):
        at = pl.multiple_of(i * LANES, LANES)
        for sub in range(LANES // TILE):
            base = pl.multiple_of(at + sub * TILE, TILE)
            for g in range(width // LANES):
                lanes = slice(g * LANES, (g + 1) * LANES)
                window = padded[pl.ds(base, TILE + REACH), lanes]
                total = jnp.zeros((TILE, LANES), jnp.float32)
                for r in range(8):
                    mine = [j for j in range(taps) if (j + skip) % 8 == r]
                    held = window[r : mine[-1] + skip + TILE]
                    for j in mine:
                        start = j + skip - r
                        total = total + taps_ref[j : j + 1, lanes] * held[start : start + TILE]
                filtered_ref[pl.ds(base, TILE), lanes] = total
        sums = jnp.zeros((LANES, LANES), jnp.float32)
        squares = jnp.zeros((LANES, LANES), jnp.float32)
        for g in range(width // LANES):
            value = filtered_ref[pl.ds(at, LANES), g * LANES : (g + 1) * LANES]
            sums = sums + value
            squares = squares + value * value
        own_stats[:, pl.ds(at, LANES)] = exact(first, sums, ((1,), (1,))) + exact(second, squares, ((1,), (1,)))
        return carry

    lax.fori_loop(0, rows // LANES, filter_tile, 0)
    stats = [
        pltpu.make_async_remote_copy(
            src_ref=own_stats, dst_ref=other_stats.at[k - 1], send_sem=stat_send.at[k - 1],
            recv_sem=stat_recv.at[k - 1], device_id={"tp": lax.rem(tp + k, groups)}, device_id_type=MESH,
        )
        for k in range(1, groups)
    ]
    for one in stats:
        one.start()
    for k, state in enumerate(states, 1):
        pl.when(me >= k)(state.wait_recv)
    for h in range(arriving_ref.shape[0]):
        arriving = jnp.zeros((head, head), jnp.float32)
        for k in range(count - 1, 0, -1):
            tail = gathered[k - 1, h, head : head + PAD, :].astype(jnp.float32)
            log = tail[0:1] + tail[1:2] + tail[2:3]
            stepped = arriving * jnp.exp(log) + gathered[k - 1, h, 0:head, :].astype(jnp.float32)
            arriving = jnp.where(me >= k, stepped, arriving)
        arriving_ref[h] = arriving.astype(jnp.bfloat16)
    for one in stats:
        one.wait_recv()
    eye = jnp.where(pick == lax.broadcasted_iota(jnp.int32, (8, LANES), 1), 1.0, 0.0)

    def stats_tile(i, carry):
        at = pl.multiple_of(i * LANES, LANES)
        total = own_stats[:, pl.ds(at, LANES)]
        for k in range(groups - 1):
            total = total + other_stats[k, :, pl.ds(at, LANES)]
        stats_ref[pl.ds(at, LANES), :] = exact(total, eye, ((0,), (0,)))
        return carry

    lax.fori_loop(0, rows // LANES, stats_tile, 0)
    edge.wait_send()
    for k, state in enumerate(states, 1):
        pl.when(me + k < count)(state.wait_send)
    for one in stats:
        one.wait_send()


def exact(a, b, dims):
    return lax.dot_general(
        a, b, (dims, ((), ())), precision=lax.Precision.HIGHEST, preferred_element_type=jnp.float32
    )


def exchange(pack, projected, conv_taps):
    heads, _, head = pack.shape
    rows, width = projected.shape[1:]
    count, groups = lax.axis_size("sp"), lax.axis_size("tp")
    whole = lambda shape: pl.BlockSpec(shape, lambda i: (0,) * len(shape))
    return pl.pallas_call(
        functools.partial(exchange_kernel, head),
        grid=(1,),
        in_specs=[
            whole(pack.shape),
            pl.BlockSpec((None, rows, width), lambda i: (4, 0, 0)),
            pl.BlockSpec((None, rows, width), lambda i: (5, 0, 0)),
            whole(conv_taps.shape),
        ],
        out_specs=[whole((heads, head, head)), whole((rows, width)), whole((rows, LANES))],
        out_shape=[
            jax.ShapeDtypeStruct((heads, head, head), jnp.bfloat16),
            jax.ShapeDtypeStruct((rows, width), jnp.float32),
            jax.ShapeDtypeStruct((rows, LANES), jnp.float32),
        ],
        scratch_shapes=[
            pltpu.VMEM((count - 1,) + pack.shape, jnp.bfloat16),
            pltpu.VMEM((2, REACH, width), jnp.bfloat16),
            pltpu.VMEM((rows + REACH, width), jnp.float32),
            pltpu.VMEM((8, rows), jnp.float32),
            pltpu.VMEM((groups - 1, 8, rows), jnp.float32),
            pltpu.SemaphoreType.DMA((count - 1,)),
            pltpu.SemaphoreType.DMA((count - 1,)),
            pltpu.SemaphoreType.DMA((2,)),
            pltpu.SemaphoreType.DMA((groups - 1,)),
            pltpu.SemaphoreType.DMA((groups - 1,)),
        ],
        compiler_params=pltpu.CompilerParams(
            dimension_semantics=("arbitrary",), collective_id=2, has_side_effects=True,
            vmem_limit_bytes=60000 * 1024,
        ),
    )(pack, projected, projected, conv_taps)


def finish_rows(head, channels, near, far, rgate, arriving, filtered, row_sum, row_square, conv_gain, head_gain):
    pieces = []
    for h in range(near.shape[1] // head):
        part = slice(h * head, (h + 1) * head)
        rec = near[:, part] + dot(far[:, part], arriving[h], ((1,), (1,)))
        rec = rec * lax.rsqrt(jnp.mean(rec * rec, axis=-1, keepdims=True) + head_epsilon) * head_gain
        gate = rgate[:, part].astype(jnp.float32)
        pieces.append((rec * (gate * jax.nn.sigmoid(gate))).astype(jnp.bfloat16))
    row_mean = row_sum / channels
    row_var = row_square / channels - row_mean * row_mean
    normed = (filtered - row_mean) * lax.rsqrt(row_var + norm_epsilon) * conv_gain
    return jnp.concatenate(pieces, axis=1), (normed * jax.nn.sigmoid(normed)).astype(jnp.bfloat16)


def finish_kernel(
    head, channels, near_ref, far_ref, rgate_ref, arriving, filtered_ref, stats_ref,
    conv_gain_ref, head_gain_ref, out_rec_ref, out_conv_ref, out_ref,
    to_pair, from_pair, to_cross, from_cross, mine, send_sem, recv_sem,
):
    pair, cross, diag, me = partners()
    greet(pair, cross)
    block = out_ref.shape[0]
    piece = block // PIECES

    def partial(owner, p):
        rows = pl.ds(pl.multiple_of(owner * block + p * piece, piece), piece)
        rec, conv = finish_rows(
            head, channels, near_ref[rows, :], far_ref[rows, :], rgate_ref[rows, :], arriving, filtered_ref[rows, :],
            stats_ref[rows, 0:1], stats_ref[rows, 1:2], conv_gain_ref[...], head_gain_ref[...],
        )
        return (dot(rec, out_rec_ref[...]) + dot(conv, out_conv_ref[...])).astype(jnp.bfloat16)

    def copy(source, target, kind, p, device):
        return pltpu.make_async_remote_copy(
            src_ref=source, dst_ref=target, send_sem=send_sem.at[kind, p], recv_sem=recv_sem.at[kind, p],
            device_id={"tp": device}, device_id_type=MESH,
        )

    started, crossing, nearby = [], [], []
    for p in range(PIECES):
        rows = pl.ds(p * piece, piece)
        to_pair[0, rows, :] = partial(diag, p)
        lent = copy(to_pair.at[0, rows, :], from_pair.at[0, rows, :], 0, p, pair)
        lent.start()
        own = partial(cross, p).astype(jnp.float32)
        lent.wait_recv()
        to_cross[rows, :] = (own + from_pair[0, rows, :].astype(jnp.float32)).astype(jnp.bfloat16)
        sent = copy(to_cross.at[rows, :], from_cross.at[rows, :], 1, p, cross)
        sent.start()
        started.append(lent)
        crossing.append(sent)
    for p in range(PIECES):
        rows = pl.ds(p * piece, piece)
        to_pair[1, rows, :] = partial(pair, p)
        lent = copy(to_pair.at[1, rows, :], from_pair.at[1, rows, :], 2, p, pair)
        lent.start()
        nearby.append(lent)
    for p in range(PIECES):
        mine[pl.ds(p * piece, piece), :] = partial(me, p).astype(jnp.float32)
    for p in range(PIECES):
        rows = pl.ds(p * piece, piece)
        nearby[p].wait_recv()
        mine[rows, :] = mine[rows, :] + from_pair[1, rows, :].astype(jnp.float32)
    for p in range(PIECES):
        rows = pl.ds(p * piece, piece)
        crossing[p].wait_recv()
        out_ref[rows, :] = (mine[rows, :] + from_cross[rows, :].astype(jnp.float32)).astype(jnp.bfloat16)
    for sent in started + crossing + nearby:
        sent.wait_send()


def finish(near, far, projected, arriving, filtered, stats, conv_gain, head_gain, out_rec, out_conv):
    rows, width = near.shape
    head = arriving.shape[2]
    columns = out_rec.shape[1]
    block = rows // lax.axis_size("tp")
    channels = filtered.shape[1] * lax.axis_size("tp")
    whole = lambda shape: pl.BlockSpec(shape, lambda i: (0,) * len(shape))
    return pl.pallas_call(
        functools.partial(finish_kernel, head, channels),
        grid=(1,),
        in_specs=[
            whole(near.shape), whole(far.shape),
            pl.BlockSpec((None, rows, width), lambda i: (3, 0, 0)),
            whole(arriving.shape), whole(filtered.shape), whole(stats.shape),
            whole((1, filtered.shape[1])), whole((1, head)), whole(out_rec.shape), whole(out_conv.shape),
        ],
        out_specs=whole((block, columns)),
        out_shape=jax.ShapeDtypeStruct((block, columns), jnp.bfloat16),
        scratch_shapes=[
            pltpu.VMEM((2, block, columns), jnp.bfloat16),
            pltpu.VMEM((2, block, columns), jnp.bfloat16),
            pltpu.VMEM((block, columns), jnp.bfloat16),
            pltpu.VMEM((block, columns), jnp.bfloat16),
            pltpu.VMEM((block, columns), jnp.float32),
            pltpu.SemaphoreType.DMA((3, PIECES)),
            pltpu.SemaphoreType.DMA((3, PIECES)),
        ],
        compiler_params=pltpu.CompilerParams(
            dimension_semantics=("arbitrary",), collective_id=1, has_side_effects=True,
            vmem_limit_bytes=60000 * 1024,
        ),
    )(near, far, projected, arriving, filtered, stats, conv_gain[None], head_gain[None], out_rec, out_conv)


def on_device(
    tokens, norm_gain, w_query, w_forget, w_value, w_rgate, w_glu_value, w_glu_gate, forget_gap,
    decay_shift, head_gain, conv_taps, conv_gain, out_rec, out_conv,
):
    weights = (w_query, w_forget, w_value, w_rgate, w_glu_value, w_glu_gate)
    projected = gather_project(tokens, norm_gain, weights)
    near, far, pack = local_scan(projected, forget_gap, decay_shift, head_gain.shape[0])
    arriving, filtered, stats = exchange(pack, projected, conv_taps)
    return finish(
        near, far, projected, arriving, filtered, stats, conv_gain, head_gain, out_rec, out_conv
    )


def solution(mesh):
    placed = (
        P(("sp", "tp"), None),
        P(),
        P(None, "tp"),
        P(None, "tp"),
        P(None, "tp"),
        P(None, "tp"),
        P(None, "tp"),
        P(None, "tp"),
        P("tp"),
        P("sp", "tp"),
        P(),
        P(None, "tp"),
        P("tp"),
        P("tp", None),
        P("tp", None),
    )
    return jax.shard_map(
        on_device, mesh=mesh, in_specs=placed, out_specs=P(("sp", "tp"), None), check_vma=False
    )
```

profile of v0, /device:TPU:25, one launch (start us, length us, event | category | flops | bytes accessed | tf_op | source)
XLA Modules:
  0.0 117.4 jit_solution(11295758948859729715)
XLA Ops:
  0.0 1.8 %copy.16.shift_ref = f32[1024,4]{1,0:T(8,128)} copy(f32[1024,4]{0,1:T(4,128)} %param.24) | data formatting | bytes 32768 | tf_op args[9]
  1.8 33.3 %shard_map.145.q_ref.f_ref.v_ref.glu_value_ref.glu_gate_ref.rgate_ref = bf16[6,1024,512]{2,1,0:T(8,128)(2,1)} custom-call(bf16[256,2048]{1,0:T(8,128)(2,1)} %tokens_ref.1, f32[1,2048]{1,0:T(1,128)} %bitcast.4, bf16[2048,512]{1,0:T(8,128)(2,1)} %w0.1, bf16[2048,512]{1,0:T(8,128)(2,1)} %w1.1, bf16[2048,512]{1,0:T(8,128)(2,1)} %w2.1, bf16[2048,512]{1,0:T(8,128)(2,1)} %w3.1, ...), custom_call_target="tpu_custom_call" | custom-call | tf_op jit(solution)/shard_map/pallas_call | solution.py:111
  35.1 11.9 %shard_map.146 = (f32[1024,512]{1,0:T(8,128)}, bf16[1024,512]{1,0:T(8,128)(2,1)}, bf16[4,144,128]{2,1,0:T(8,128)(2,1)}) custom-call(bf16[6,1024,512]{2,1,0:T(8,128)(2,1)} %shard_map.145.q_ref.f_ref.v_ref.glu_value_ref.glu_gate_ref.rgate_ref, bf16[6,1024,512]{2,1,0:T(8,128)(2,1)} %shard_map.145.q_ref.f_ref.v_ref.glu_value_ref.glu_gate_ref.rgate_ref, ...), custom_call_target="tpu_custom_call" | custom-call | flops 805306368 | bytes 6291456 | tf_op jit(solution)/shard_map/pallas_call | solution.py:195
  47.0 31.8 %shard_map.147 = (bf16[4,128,128]{2,1,0:T(8,128)(2,1)}, f32[1024,512]{1,0:T(8,128)}, f32[1024,128]{1,0:T(8,128)}) custom-call(bf16[4,144,128]{2,1,0:T(8,128)(2,1)} %get-tuple-element.13.pack_ref, bf16[6,1024,512]{2,1,0:T(8,128)(2,1)} %shard_map.145.q_ref.f_ref.v_ref.glu_value_ref.glu_gate_ref.rgate_ref, ...), custom_call_target="tpu_custom_call" | custom-call | tf_op jit(solution)/shard_map/pallas_call | solution.py:348
  78.8 36.3 %shard_map.148 = bf16[256,2048]{1,0:T(8,128)(2,1)} custom-call(f32[1024,512]{1,0:T(8,128)} %get-tuple-element.11.near_ref, bf16[1024,512]{1,0:T(8,128)(2,1)} %get-tuple-element.12.far_ref, bf16[6,1024,512]{2,1,0:T(8,128)(2,1)} %shard_map.145.q_ref.f_ref.v_ref.glu_value_ref.glu_gate_ref.rgate_ref, bf16[4,128,128]{2,1,0:T(8,128)(2,1)} %get-tuple-element.14.arriving, ...), custom_call_target="tpu_custom_call" | custom-call | tf_op jit(solution)/shard_map/pallas_call | solution.py:460
  115.1 2.3 %copy.18 = bf16[256,2048]{1,0:T(8,128)(2,1)} copy(bf16[256,2048]{1,0:T(8,128)(2,1)} %shard_map.148) | data formatting | bytes 2097152
where the time goes:
time: 119 us; the launch traced here: 117 us
  Pallas kernels  113 us (95%)
  local copies, waits for them, and re-layouts  4.1 us (3%)
    pallas_call x1, Pallas kernels, finish(): pl.pallas_call(functools.partial(finish_kernel, head, channels), grid=(1,...  36.3 us
    pallas_call x1, Pallas kernels, gather_project(): pl.pallas_call(project_kernel, in_specs=[pl.BlockSpec(memory_space=pltpu....  33.3 us
    pallas_call x1, Pallas kernels, exchange(): pl.pallas_call(functools.partial(exchange_kernel, head), grid=(1,), in_sp...  31.8 us
    pallas_call x1, Pallas kernels, local_scan(): pl.pallas_call(functools.partial(scan_kernel, head), grid=(rows // CHUNK,...  11.9 us
    unnamed x2, local copies, waits for them, and re-layouts  4.1 us

commit v1 on v0

v1 whole, which is shorter than its diff:
```python
import functools

import jax
import jax.numpy as jnp
from jax import lax
from jax.experimental import pallas as pl
from jax.experimental.pallas import tpu as pltpu
from jax.sharding import PartitionSpec as P

CHUNK = 128
PAD = 16
SENDS = 4
RETURNS = 4
REACH = 32
TILE = 64
LANES = 128
SPAN = 512
MESH = pl.DeviceIdType.MESH
FORGET, VALUE, QUERY, GLU_VALUE, GLU_GATE, RGATE = range(6)

norm_epsilon = 1e-05
head_epsilon = 1e-06


def dot(a, b, dims=((1,), (0,))):
    return lax.dot_general(a, b, (dims, ((), ())), preferred_element_type=jnp.float32)


def exact(a, b, dims):
    return lax.dot_general(
        a, b, (dims, ((), ())), precision=lax.Precision.HIGHEST, preferred_element_type=jnp.float32
    )


def layer_norm(values, gain):
    widened = values.astype(jnp.float32)
    row_mean = jnp.mean(widened, axis=-1, keepdims=True)
    centred = widened - row_mean
    row_var = jnp.mean(centred * centred, axis=-1, keepdims=True)
    return centred * lax.rsqrt(row_var + norm_epsilon) * gain


def layer_kernel(
    head, tokens_ref, gain_ref, gap_ref, shift_ref, taps_ref, conv_gain_ref, head_gain_ref,
    w0, w1, w2, w3, w4, w5, rec_rows, conv_rows, out_ref,
    near_rows, far_rows, weight, merge, proj, intra, reach, local, closing, enter,
    own_state, own_log, pack, pack_in, group_state, group_log, chain_out, chain_in,
    rim, padded, filtered, own_stats, other_stats, moments,
    blend, held, to_pair, from_pair, to_cross, from_cross, mine, done,
    weight_sem, send_sem, recv_sem, pack_send, pack_recv, chain_send, chain_recv,
    rim_sem, stat_send, stat_recv, back_send, back_recv, out_sem,
):
    sources = (w0, w1, w2, w3, w4, w5)
    width = gap_ref.shape[1]
    fetched = [pltpu.make_async_copy(w, weight.at[i], weight_sem.at[i]) for i, w in enumerate(sources)]
    for i, w in enumerate((rec_rows, conv_rows)):
        fetched.append(
            pltpu.make_async_copy(w, merge.at[pl.ds(i * width, width), :], weight_sem.at[len(sources) + i])
        )
    for one in fetched:
        one.start()

    me, count = lax.axis_index("tp"), lax.axis_size("sp")
    pair = me + 1 - 2 * lax.rem(me, 2)
    cross, diag = lax.rem(me + 2, 4), lax.rem(pair + 2, 4)
    at = lax.axis_index("sp")
    side, team, teams = lax.rem(at, 2), at // 2, count // 2
    mate = at + 1 - 2 * side
    barrier = pltpu.get_barrier_semaphore()
    for other in (pair, cross, diag):
        pl.semaphore_signal(barrier, inc=1, device_id={"tp": other}, device_id_type=MESH)
    for hop in (1, 2, count - 1, count - 2):
        pl.semaphore_signal(barrier, inc=1, device_id={"sp": lax.rem(at + hop, count)}, device_id_type=MESH)
    pl.semaphore_wait(barrier, 7)

    block, depth = tokens_ref.shape
    rows_all = proj.shape[1]
    heads, chunks = width // head, rows_all // CHUNK
    piece = block // SENDS
    bigs = block // CHUNK
    per = CHUNK // piece
    lanes_of = [slice(g * LANES, (g + 1) * LANES) for g in range(width // LANES)]

    def remote(source, target, sends, recvs, axis, device):
        return pltpu.make_async_remote_copy(
            src_ref=source, dst_ref=target, send_sem=sends, recv_sem=recvs,
            device_id={axis: device}, device_id_type=MESH,
        )

    crossing, nearby, handed = [], [], []
    for p in range(SENDS):
        rows = pl.ds(p * piece, piece)
        near_rows[0, rows, :] = layer_norm(tokens_ref[rows, :], gain_ref[...]).astype(jnp.bfloat16)
        big, low = p // per, (p % per) * piece
        landing = far_rows.at[big, pl.ds(low, piece), :]
        crossing.append(remote(near_rows.at[0, rows, :], landing, send_sem.at[0, p], recv_sem.at[0, p], "tp", cross))
        nearby.append(
            remote(
                near_rows.at[0, rows, :], near_rows.at[1, rows, :], send_sem.at[1, p], recv_sem.at[1, p], "tp", pair
            )
        )
        handed.append(
            remote(
                landing, far_rows.at[big, pl.ds(CHUNK + low, piece), :],
                send_sem.at[2, p], recv_sem.at[2, p], "tp", pair,
            )
        )
        crossing[p].start()
        nearby[p].start()

    def project(values, first, last, places, ready=False):
        def step(i, carry):
            if ready:
                for k in range(first, last):
                    pl.when(i == k)(fetched[k].wait)
            result = dot(values[...], weight[i]).astype(jnp.bfloat16)
            for start, row, size in places:
                proj[i, pl.ds(pl.multiple_of(row, CHUNK), size), :] = result[start : start + size]
            return carry

        lax.fori_loop(first, last, step, 0)

    def pass_on(p):
        crossing[p].wait_recv()
        handed[p].start()

    row_at = lax.broadcasted_iota(jnp.int32, (CHUNK, CHUNK), 0)
    col_at = lax.broadcasted_iota(jnp.int32, (CHUNK, CHUNK), 1)
    causal = row_at >= col_at
    lower = jnp.where(causal, 1.0, 0.0).astype(jnp.bfloat16)
    lower = jnp.concatenate([lower, lower], axis=1)

    def chunk(c):
        rows = pl.ds(pl.multiple_of(c * CHUNK, CHUNK), CHUNK)
        for h in range(heads):
            part = slice(h * head, (h + 1) * head)
            query = proj[QUERY, rows, part].astype(jnp.float32)
            query = query * jax.nn.sigmoid(query)
            key = gap_ref[:, part] * jax.nn.sigmoid(-proj[FORGET, rows, part].astype(jnp.float32))
            shift = jnp.broadcast_to(shift_ref[h : h + 1, rows], (head, CHUNK)).T
            log = jnp.log1p(-key) + shift
            value = proj[VALUE, rows, part]
            high = log.astype(jnp.bfloat16)
            low = (log - high.astype(jnp.float32)).astype(jnp.bfloat16)
            total = dot(lower, jnp.concatenate([high, low], axis=0))
            last = total[CHUNK - 1 : CHUNK, :]
            middle = total[CHUNK // 2 - 1 : CHUNK // 2, :]
            query_mid = query * jnp.exp(total - middle)
            key_mid = key * jnp.exp(middle - total)
            scores = dot(query_mid.astype(jnp.bfloat16), key_mid.astype(jnp.bfloat16), ((1,), (1,)))
            scores = jnp.where(causal, scores, 0.0).astype(jnp.bfloat16)
            intra[rows, part] = dot(scores, value)
            reach[rows, part] = (query_mid * jnp.exp(middle)).astype(jnp.bfloat16)
            key_end = (key_mid * jnp.exp(last - middle)).astype(jnp.bfloat16)
            local[c, h] = dot(value, key_end, ((0,), (0,)))
            closing[c, :, part] = last

    def chunk_loop(first, number):
        def step(i, carry):
            chunk(first + i)
            return carry

        lax.fori_loop(0, number, step, 0)

    def mix(first, size):
        def step(i, carry):
            row = pl.multiple_of(first + i * TILE, TILE)
            for g, lanes in enumerate(lanes_of):
                gate = proj[GLU_GATE, pl.ds(row, TILE), lanes].astype(jnp.float32)
                value = proj[GLU_VALUE, pl.ds(row, TILE), lanes].astype(jnp.float32)
                mixed = (value * jax.nn.sigmoid(gate)).astype(jnp.bfloat16)
                padded[g, pl.ds(pl.multiple_of(row + REACH, 8), TILE), :] = mixed.astype(jnp.float32)
            return carry

        lax.fori_loop(0, size // TILE, step, 0)

    taps = taps_ref.shape[0]
    skip = REACH - taps + 1
    pick = lax.broadcasted_iota(jnp.int32, (8, LANES), 0)
    one_hot = [jnp.where(pick == k, 1.0, 0.0) for k in range(2)]

    def filter_tile(t):
        base = pl.multiple_of(t * LANES, LANES)

        def step(i, carry):
            g, row = i // (LANES // TILE), base + lax.rem(i, LANES // TILE) * TILE
            lanes = pl.ds(pl.multiple_of(g * LANES, LANES), LANES)
            total = jnp.zeros((TILE, LANES), jnp.float32)
            for j in range(taps):
                total = total + taps_ref[j : j + 1, lanes] * padded[g, pl.ds(row + (j + skip), TILE), :]
            filtered[pl.ds(pl.multiple_of(row, TILE), TILE), lanes] = total
            return carry

        lax.fori_loop(0, len(lanes_of) * (LANES // TILE), step, 0)
        sums = jnp.zeros((LANES, LANES), jnp.float32)
        squares = jnp.zeros((LANES, LANES), jnp.float32)
        for lanes in lanes_of:
            value = filtered[pl.ds(base, LANES), lanes]
            sums = sums + value
            squares = squares + value * value
        own_stats[:, pl.ds(base, LANES)] = exact(one_hot[0], sums, ((1,), (1,))) + exact(
            one_hot[1], squares, ((1,), (1,))
        )

    def filter_loop(first, number):
        def step(i, carry):
            filter_tile(first + i)
            return carry

        lax.fori_loop(0, number, step, 0)

    chip = 2 * block
    own_half = (me // 2) * chip
    far_half = chip - own_half if rows_all == 2 * chip else lax.rem(own_half + chip, rows_all)
    half_tiles = chip // LANES

    project(near_rows.at[0], 0, len(sources), [(0, me * block, block)], ready=True)
    for one in nearby:
        one.wait_recv()
    project(near_rows.at[1], 0, len(sources), [(0, pair * block, block)])
    pass_on(0)
    chunk_loop(own_half // CHUNK, chip // CHUNK)
    pass_on(1)
    mix(own_half, chip)
    filter_loop(own_half // LANES + 1, half_tiles - 1)

    def far_places(big):
        return [(0, cross * block + big * CHUNK, CHUNK), (CHUNK, diag * block + big * CHUNK, CHUNK)]

    def far_chunks(big):
        def step(i, carry):
            chunk(jnp.where(i == 0, cross, diag) * bigs + big)
            return carry

        lax.fori_loop(0, 2, step, 0)

    for big in range(bigs):
        final = big == bigs - 1
        for p in range(big * per, (big + 1) * per):
            if p > 1:
                pass_on(p)
        for p in range(big * per, (big + 1) * per):
            handed[p].wait_recv()
        if final:
            project(far_rows.at[big], 0, 3, far_places(big))
            far_chunks(big)
        else:
            project(far_rows.at[big], 0, len(sources), far_places(big))
            far_chunks(big)
            for _, row, size in far_places(big):
                mix(row, size)

    place = lax.broadcasted_iota(jnp.int32, (PAD, head), 0)
    packs = [remote(pack.at[h], pack_in.at[h], pack_send.at[h], pack_recv.at[h], "sp", mate) for h in range(heads)]
    for h in range(heads):
        part = slice(h * head, (h + 1) * head)
        state, log = local[0, h], closing[0, :, part]
        for c in range(1, chunks):
            state = state * jnp.exp(closing[c, :, part]) + local[c, h]
            log = log + closing[c, :, part]
        own_state[h] = state
        own_log[:, part] = log
        pack[h, 0:head, :] = state.astype(jnp.bfloat16)
        high = log.astype(jnp.bfloat16).astype(jnp.float32)
        rest = log - high
        mid = rest.astype(jnp.bfloat16).astype(jnp.float32)
        low = rest - mid
        tail = jnp.where(place == 0, high, jnp.where(place == 1, mid, jnp.where(place == 2, low, 0.0)))
        pack[h, head : head + PAD, :] = tail.astype(jnp.bfloat16)
        packs[h].start()

    project(far_rows.at[bigs - 1], 3, len(sources), far_places(bigs - 1))
    for _, row, size in far_places(bigs - 1):
        mix(row, size)
    for g, lanes in enumerate(lanes_of):
        rim[0, :, lanes] = padded[g, rows_all : rows_all + REACH, :].astype(jnp.bfloat16)
    edge = remote(rim.at[0], rim.at[1], rim_sem.at[0], rim_sem.at[1], "sp", lax.rem(at + 1, count))
    edge.start()

    links = [
        remote(chain_out.at[h], chain_in.at[h], chain_send.at[h], chain_recv.at[h], "sp", lax.rem(at + 2, count))
        for h in range(heads)
    ]

    def mate_log(h):
        tail = pack_in[h, head : head + PAD, :].astype(jnp.float32)
        return tail[0:1] + tail[1:2] + tail[2:3]

    for h in range(heads):
        part = slice(h * head, (h + 1) * head)
        packs[h].wait_recv()
        theirs, log = pack_in[h, 0:head, :].astype(jnp.float32), mate_log(h)
        ours, own = own_state[h], own_log[:, part]
        first = jnp.where(side == 0, ours, theirs)
        second = jnp.where(side == 0, theirs, ours)
        group_state[h] = first * jnp.exp(jnp.where(side == 0, log, own)) + second
        group_log[:, part] = log + own

        @pl.when(team == 0)
        def _():
            chain_in[h] = jnp.zeros((head, head), jnp.bfloat16)
            chain_out[h] = group_state[h].astype(jnp.bfloat16)
            links[h].start()

    def relay(k):
        @pl.when(team == k)
        def _():
            for h in range(heads):
                links[h].wait_recv()
                if k < teams - 1:
                    part = slice(h * head, (h + 1) * head)
                    step = chain_in[h].astype(jnp.float32) * jnp.exp(group_log[:, part]) + group_state[h]
                    chain_out[h] = step.astype(jnp.bfloat16)
                    links[h].start()

    far_tile = far_half // LANES

    def rim_in():
        edge.wait_recv()
        for g, lanes in enumerate(lanes_of):
            padded[g, 0:REACH, :] = jnp.where(at > 0, rim[1, :, lanes].astype(jnp.float32), 0.0)
        filter_tile(own_half // LANES)

    stats = [
        remote(own_stats, other_stats.at[k - 1], stat_send.at[k - 1], stat_recv.at[k - 1], "tp", lax.rem(me + k, 4))
        for k in range(1, 4)
    ]

    def send_stats():
        filter_tile(far_tile)
        for one in stats:
            one.start()

    work = [lambda: filter_loop(far_tile + 1, 2), lambda: filter_loop(far_tile + 3, 1), rim_in, send_stats]
    if half_tiles != 4:
        work[1] = lambda: filter_loop(far_tile + 3, half_tiles - 3)
    relays = [functools.partial(relay, k) for k in range(1, teams)]
    while work or relays:
        if work:
            work.pop(0)()
        if relays:
            relays.pop(0)()

    eye = jnp.where(pick == lax.broadcasted_iota(jnp.int32, (8, LANES), 1), 1.0, 0.0)
    for one in stats:
        one.wait_recv()

    def stats_tile(i, carry):
        row = pl.multiple_of(i * LANES, LANES)
        total = own_stats[:, pl.ds(row, LANES)]
        for k in range(3):
            total = total + other_stats[k, :, pl.ds(row, LANES)]
        moments[pl.ds(row, LANES), :] = exact(total, eye, ((0,), (0,)))
        return carry

    lax.fori_loop(0, rows_all // LANES, stats_tile, 0)

    for h in range(heads):
        part = slice(h * head, (h + 1) * head)
        state = chain_in[h].astype(jnp.float32)
        moved = state * jnp.exp(mate_log(h)) + pack_in[h, 0:head, :].astype(jnp.float32)
        state = jnp.where(side == 1, moved, state)
        for c in range(chunks):
            enter[c, h] = state.astype(jnp.bfloat16)
            if c < chunks - 1:
                state = state * jnp.exp(closing[c, :, part]) + local[c, h]

    channels = width * lax.axis_size("tp")

    def finish_rows(owner, low, size, slot):
        start = pl.multiple_of(owner * block + low, size)
        rows, c = pl.ds(start, size), owner * bigs + low // CHUNK
        target = pl.ds(slot, size)
        for h in range(heads):
            part = slice(h * head, (h + 1) * head)
            rec = intra[rows, part] + dot(reach[rows, part], enter[c, h], ((1,), (1,)))
            rec = rec * lax.rsqrt(jnp.mean(rec * rec, axis=-1, keepdims=True) + head_epsilon) * head_gain_ref[...]
            gate = proj[RGATE, rows, part].astype(jnp.float32)
            blend[target, part] = (rec * (gate * jax.nn.sigmoid(gate))).astype(jnp.bfloat16)
        row_mean = moments[rows, 0:1] / channels
        row_var = moments[rows, 1:2] / channels - row_mean * row_mean
        scale = lax.rsqrt(row_var + norm_epsilon)
        for g, lanes in enumerate(lanes_of):
            normed = (filtered[rows, lanes] - row_mean) * scale * conv_gain_ref[:, lanes]
            blend[target, width + g * LANES : width + (g + 1) * LANES] = (normed * jax.nn.sigmoid(normed)).astype(
                jnp.bfloat16
            )

    columns = merge.shape[1]

    def spread(size, put):
        def step(j, carry):
            cols = pl.ds(pl.multiple_of(j * SPAN, SPAN), SPAN)
            put(cols, dot(blend[0:size, :], merge[:, cols]))
            return carry

        lax.fori_loop(0, columns // SPAN, step, 0)

    for one in fetched[len(sources) :]:
        one.wait()
    turn = block // RETURNS
    lent, returned, close = [], [], []

    def settle(p):
        rows = pl.ds(p * turn, turn)
        lent[p].wait_recv()
        to_cross[rows, :] = (held[p % 2] + from_pair[0, rows, :].astype(jnp.float32)).astype(jnp.bfloat16)
        returned.append(
            remote(to_cross.at[rows, :], from_cross.at[rows, :], back_send.at[1, p], back_recv.at[1, p], "tp", cross)
        )
        returned[p].start()

    for p in range(RETURNS):
        rows = pl.ds(p * turn, turn)
        finish_rows(diag, p * turn, turn, 0)
        finish_rows(cross, p * turn, turn, turn)

        def put(cols, result, p=p, rows=rows):
            to_pair[0, rows, cols] = result[0:turn].astype(jnp.bfloat16)
            held[p % 2, :, cols] = result[turn : 2 * turn]

        spread(2 * turn, put)
        lent.append(
            remote(
                to_pair.at[0, rows, :], from_pair.at[0, rows, :], back_send.at[0, p], back_recv.at[0, p], "tp", pair
            )
        )
        lent[p].start()
        if p > 0:
            settle(p - 1)
    settle(RETURNS - 1)
    for big in range(bigs):
        rows = pl.ds(big * CHUNK, CHUNK)
        finish_rows(pair, big * CHUNK, CHUNK, 0)
        finish_rows(me, big * CHUNK, CHUNK, CHUNK)

        def put(cols, result, rows=rows):
            to_pair[1, rows, cols] = result[0:CHUNK].astype(jnp.bfloat16)
            mine[rows, cols] = result[CHUNK : 2 * CHUNK]

        spread(2 * CHUNK, put)
        close.append(
            remote(
                to_pair.at[1, rows, :], from_pair.at[1, rows, :], back_send.at[2, big], back_recv.at[2, big],
                "tp", pair,
            )
        )
        close[big].start()
    for big in range(bigs):
        rows = pl.ds(big * CHUNK, CHUNK)
        close[big].wait_recv()
        mine[rows, :] = mine[rows, :] + from_pair[1, rows, :].astype(jnp.float32)
    stores = []
    for p in range(RETURNS):
        rows = pl.ds(p * turn, turn)
        returned[p].wait_recv()
        done[rows, :] = (mine[rows, :] + from_cross[rows, :].astype(jnp.float32)).astype(jnp.bfloat16)
        stores.append(pltpu.make_async_copy(done.at[rows, :], out_ref.at[rows, :], out_sem.at[p]))
        stores[p].start()
    for one in crossing + nearby + handed + packs + [edge] + stats + lent + returned + close:
        one.wait_send()

    @pl.when(team < teams - 1)
    def _():
        for one in links:
            one.wait_send()

    for one in stores:
        one.wait()


def on_device(
    tokens, norm_gain, w_query, w_forget, w_value, w_rgate, w_glu_value, w_glu_gate, forget_gap,
    decay_shift, head_gain, conv_taps, conv_gain, out_rec, out_conv,
):
    weights = (w_forget, w_value, w_query, w_glu_value, w_glu_gate, w_rgate)
    block, depth = tokens.shape
    width, columns = out_rec.shape
    head = head_gain.shape[0]
    heads = width // head
    rows = block * lax.axis_size("tp")
    groups = width // LANES
    chunks = rows // CHUNK
    turn = block // RETURNS
    bf16, f32 = jnp.bfloat16, jnp.float32
    vmem = lambda shape, kind: pltpu.VMEM(shape, kind)
    sems = lambda *shape: pltpu.SemaphoreType.DMA(shape)
    return pl.pallas_call(
        functools.partial(layer_kernel, head),
        in_specs=[pl.BlockSpec(memory_space=pltpu.VMEM)] * 7 + [pl.BlockSpec(memory_space=pl.ANY)] * 8,
        out_specs=pl.BlockSpec(memory_space=pl.ANY),
        out_shape=jax.ShapeDtypeStruct((block, columns), bf16),
        scratch_shapes=[
            vmem((2, block, depth), bf16),
            vmem((block // CHUNK, 2 * CHUNK, depth), bf16),
            vmem((len(weights), depth, width), bf16),
            vmem((2 * width, columns), bf16),
            vmem((len(weights), rows, width), bf16),
            vmem((rows, width), f32),
            vmem((rows, width), bf16),
            vmem((chunks, heads, head, head), f32),
            vmem((chunks, 1, width), f32),
            vmem((chunks, heads, head, head), bf16),
            vmem((heads, head, head), f32),
            vmem((1, width), f32),
            vmem((heads, head + PAD, head), bf16),
            vmem((heads, head + PAD, head), bf16),
            vmem((heads, head, head), f32),
            vmem((1, width), f32),
            vmem((heads, head, head), bf16),
            vmem((heads, head, head), bf16),
            vmem((2, REACH, width), bf16),
            vmem((groups, REACH + rows, LANES), f32),
            vmem((rows, width), f32),
            vmem((8, rows), f32),
            vmem((3, 8, rows), f32),
            vmem((rows, LANES), f32),
            vmem((2 * CHUNK, 2 * width), bf16),
            vmem((2, turn, columns), f32),
            vmem((2, block, columns), bf16),
            vmem((2, block, columns), bf16),
            vmem((block, columns), bf16),
            vmem((block, columns), bf16),
            vmem((block, columns), f32),
            vmem((block, columns), bf16),
            sems(len(weights) + 2),
            sems(3, SENDS),
            sems(3, SENDS),
            sems(heads),
            sems(heads),
            sems(heads),
            sems(heads),
            sems(2),
            sems(3),
            sems(3),
            sems(3, RETURNS),
            sems(3, RETURNS),
            sems(RETURNS),
        ],
        compiler_params=pltpu.CompilerParams(
            collective_id=0, has_side_effects=True, vmem_limit_bytes=65000 * 1024
        ),
    )(
        tokens, norm_gain[None], forget_gap[None], decay_shift.T, conv_taps, conv_gain[None], head_gain[None],
        *weights, out_rec, out_conv,
    )


def solution(mesh):
    placed = (
        P(("sp", "tp"), None),
        P(),
        P(None, "tp"),
        P(None, "tp"),
        P(None, "tp"),
        P(None, "tp"),
        P(None, "tp"),
        P(None, "tp"),
        P("tp"),
        P("sp", "tp"),
        P(),
        P(None, "tp"),
        P("tp"),
        P("tp", None),
        P("tp", None),
    )
    return jax.shard_map(
        on_device, mesh=mesh, in_specs=placed, out_specs=P(("sp", "tp"), None), check_vma=False
    )
```

time: 119 us -> 89.5 us (0.75)
  Pallas kernels: 113 us -> 86.3 us
  local copies, waits for them, and re-layouts: 4.1 us -> 2.3 us
    pallas_call x4 -> x1, Pallas kernels: 113 us -> 86.3 us  [on_device(): pl.pallas_call(functools.partial(layer_kernel, head), in_specs=[pl.BlockS...]
    unnamed x2 -> x1, local copies, waits for them, and re-layouts: 4.1 us -> 2.3 us
where the time goes in v1:
time: 89.5 us; the launch traced here: 88.6 us
  Pallas kernels  86.3 us (96%)
  local copies, waits for them, and re-layouts  2.3 us (3%)
    pallas_call x1, Pallas kernels, on_device(): pl.pallas_call(functools.partial(layer_kernel, head), in_specs=[pl.BlockS...  86.3 us
    unnamed x1, local copies, waits for them, and re-layouts  2.3 us

profile of v1, /device:TPU:25, one launch (start us, length us, event | category | flops | bytes accessed | tf_op | source)
XLA Modules:
  0.0 88.6 jit_solution(17368363158030437340)
XLA Ops:
  0.0 86.3 %shard_map.145 = bf16[256,2048]{1,0:T(8,128)(2,1)} custom-call(bf16[256,2048]{1,0:T(8,128)(2,1)} %tokens_ref.1, f32[1,2048]{1,0:T(1,128)} %bitcast.6, f32[1,512]{1,0:T(1,128)} %bitcast.7, f32[4,1024]{1,0:T(4,128)} %bitcast.5, f32[31,512]{1,0:T(8,128)} %taps_ref.1, f32[1,512]{1,0:T(1,128)} %bitcast.8, f32[1,128]{1,0:T(1,128)} %bitcast.9, ...), custom_call_target="tpu_custom_call" | custom-call | tf_op jit(solution)/shard_map/pallas_call | solution.py:488
  86.3 2.3 %copy.17 = bf16[256,2048]{1,0:T(8,128)(2,1)} copy(bf16[256,2048]{1,0:T(8,128)(2,1)} %shard_map.145) | data formatting | bytes 2097152

commit v2 on v1

--- a/solution.py
+++ b/solution.py
@@ -26,12 +26,6 @@
     return lax.dot_general(a, b, (dims, ((), ())), preferred_element_type=jnp.float32)
 
 
-def exact(a, b, dims):
-    return lax.dot_general(
-        a, b, (dims, ((), ())), precision=lax.Precision.HIGHEST, preferred_element_type=jnp.float32
-    )
-
-
 def layer_norm(values, gain):
     widened = values.astype(jnp.float32)
     row_mean = jnp.mean(widened, axis=-1, keepdims=True)
@@ -41,15 +35,22 @@
 
 
 def layer_kernel(
-    head, tokens_ref, gain_ref, gap_ref, shift_ref, taps_ref, conv_gain_ref, head_gain_ref,
-    w0, w1, w2, w3, w4, w5, rec_rows, conv_rows, out_ref,
-    near_rows, far_rows, weight, merge, proj, intra, reach, local, closing, enter,
+    head, gain_ref, gap_ref, shift_ref, taps_ref, conv_gain_ref, head_gain_ref,
+    tokens_ref, w0, w1, w2, w3, w4, w5, rec_rows, conv_rows, out_ref,
+    raw, near_rows, far_rows, weight, merge, proj, intra, reach, local, closing, centre, enter,
     own_state, own_log, pack, pack_in, group_state, group_log, chain_out, chain_in,
     rim, padded, filtered, own_stats, other_stats, moments,
     blend, held, to_pair, from_pair, to_cross, from_cross, mine, done,
-    weight_sem, send_sem, recv_sem, pack_send, pack_recv, chain_send, chain_recv,
+    raw_sem, weight_sem, send_sem, recv_sem, pack_send, pack_recv, chain_send, chain_recv,
     rim_sem, stat_send, stat_recv, back_send, back_recv, out_sem,
 ):
+    block, depth = tokens_ref.shape
+    piece = block // SENDS
+    raws = []
+    for p in range(SENDS):
+        rows = pl.ds(p * piece, piece)
+        raws.append(pltpu.make_async_copy(tokens_ref.at[rows, :], raw.at[rows, :], raw_sem.at[p]))
+        raws[p].start()
     sources = (w0, w1, w2, w3, w4, w5)
     width = gap_ref.shape[1]
     fetched = [pltpu.make_async_copy(w, weight.at[i], weight_sem.at[i]) for i, w in enumerate(sources)]
@@ -57,9 +58,6 @@
         fetched.append(
             pltpu.make_async_copy(w, merge.at[pl.ds(i * width, width), :], weight_sem.at[len(sources) + i])
         )
-    for one in fetched:
-        one.start()
-
     me, count = lax.axis_index("tp"), lax.axis_size("sp")
     pair = me + 1 - 2 * lax.rem(me, 2)
     cross, diag = lax.rem(me + 2, 4), lax.rem(pair + 2, 4)
@@ -73,12 +71,11 @@
         pl.semaphore_signal(barrier, inc=1, device_id={"sp": lax.rem(at + hop, count)}, device_id_type=MESH)
     pl.semaphore_wait(barrier, 7)
 
-    block, depth = tokens_ref.shape
     rows_all = proj.shape[1]
     heads, chunks = width // head, rows_all // CHUNK
-    piece = block // SENDS
     bigs = block // CHUNK
     per = CHUNK // piece
+    channels = width * lax.axis_size("tp")
     lanes_of = [slice(g * LANES, (g + 1) * LANES) for g in range(width // LANES)]
 
     def remote(source, target, sends, recvs, axis, device):
@@ -87,10 +84,15 @@
             device_id={axis: device}, device_id_type=MESH,
         )
 
+    for one in raws:
+        one.wait()
+    for one in fetched:
+        one.start()
+
     crossing, nearby, handed = [], [], []
     for p in range(SENDS):
         rows = pl.ds(p * piece, piece)
-        near_rows[0, rows, :] = layer_norm(tokens_ref[rows, :], gain_ref[...]).astype(jnp.bfloat16)
+        near_rows[0, rows, :] = layer_norm(raw[rows, :], gain_ref[...]).astype(jnp.bfloat16)
         big, low = p // per, (p % per) * piece
         landing = far_rows.at[big, pl.ds(low, piece), :]
         crossing.append(remote(near_rows.at[0, rows, :], landing, send_sem.at[0, p], recv_sem.at[0, p], "tp", cross))
@@ -109,16 +111,18 @@
         nearby[p].start()
 
     def project(values, first, last, places, ready=False):
-        def step(i, carry):
-            if ready:
-                for k in range(first, last):
-                    pl.when(i == k)(fetched[k].wait)
-            result = dot(values[...], weight[i]).astype(jnp.bfloat16)
-            for start, row, size in places:
-                proj[i, pl.ds(pl.multiple_of(row, CHUNK), size), :] = result[start : start + size]
+        def step(k, carry):
+            for i in (first + 2 * k, first + 2 * k + 1):
+                if ready:
+                    for one in range(first, last):
+                        pl.when(i == one)(fetched[one].wait)
+            for i in (first + 2 * k, first + 2 * k + 1):
+                result = dot(values[...], weight[i]).astype(jnp.bfloat16)
+                for start, row, size in places:
+                    proj[i, pl.ds(pl.multiple_of(row, CHUNK), size), :] = result[start : start + size]
             return carry
 
-        lax.fori_loop(first, last, step, 0)
+        lax.fori_loop(0, (last - first) // 2, step, 0)
 
     def pass_on(p):
         crossing[p].wait_recv()
@@ -130,37 +134,60 @@
     lower = jnp.where(causal, 1.0, 0.0).astype(jnp.bfloat16)
     lower = jnp.concatenate([lower, lower], axis=1)
 
-    def chunk(c):
-        rows = pl.ds(pl.multiple_of(c * CHUNK, CHUNK), CHUNK)
-        for h in range(heads):
-            part = slice(h * head, (h + 1) * head)
-            query = proj[QUERY, rows, part].astype(jnp.float32)
-            query = query * jax.nn.sigmoid(query)
-            key = gap_ref[:, part] * jax.nn.sigmoid(-proj[FORGET, rows, part].astype(jnp.float32))
-            shift = jnp.broadcast_to(shift_ref[h : h + 1, rows], (head, CHUNK)).T
-            log = jnp.log1p(-key) + shift
-            value = proj[VALUE, rows, part]
+    parts = [slice(h * head, (h + 1) * head) for h in range(heads)]
+
+    def rows_of(c):
+        return pl.ds(pl.multiple_of(c * CHUNK, CHUNK), CHUNK)
+
+    def state_part(several):
+        keys, totals = [], []
+        for c in several:
+            rows = rows_of(c)
+            key = gap_ref[...] * jax.nn.sigmoid(-proj[FORGET, rows, :].astype(jnp.float32))
+            shift = [jnp.broadcast_to(shift_ref[h : h + 1, rows], (head, CHUNK)).T for h in range(heads)]
+            log = jnp.log1p(-key) + jnp.concatenate(shift, axis=1)
             high = log.astype(jnp.bfloat16)
             low = (log - high.astype(jnp.float32)).astype(jnp.bfloat16)
-            total = dot(lower, jnp.concatenate([high, low], axis=0))
+            keys.append(key)
+            totals.append(dot(lower, jnp.concatenate([high, low], axis=0)))
+        for c, key, total in zip(several, keys, totals):
+            rows = rows_of(c)
             last = total[CHUNK - 1 : CHUNK, :]
             middle = total[CHUNK // 2 - 1 : CHUNK // 2, :]
-            query_mid = query * jnp.exp(total - middle)
-            key_mid = key * jnp.exp(middle - total)
-            scores = dot(query_mid.astype(jnp.bfloat16), key_mid.astype(jnp.bfloat16), ((1,), (1,)))
-            scores = jnp.where(causal, scores, 0.0).astype(jnp.bfloat16)
-            intra[rows, part] = dot(scores, value)
-            reach[rows, part] = (query_mid * jnp.exp(middle)).astype(jnp.bfloat16)
+            total = total - middle
+            key_mid = key * jnp.exp(-total)
+            intra[rows, :] = total
+            reach[rows, :] = key_mid.astype(jnp.bfloat16)
             key_end = (key_mid * jnp.exp(last - middle)).astype(jnp.bfloat16)
-            local[c, h] = dot(value, key_end, ((0,), (0,)))
-            closing[c, :, part] = last
+            for h, part in enumerate(parts):
+                local[c, h] = dot(proj[VALUE, rows, part], key_end[:, part], ((0,), (0,)))
+            closing[c] = last
+            centre[c] = middle
+
+    def query_part(several):
+        queries, scores = [], []
+        for c in several:
+            rows = rows_of(c)
+            query = proj[QUERY, rows, :].astype(jnp.float32)
+            query = query * jax.nn.sigmoid(query) * jnp.exp(intra[rows, :])
+            queries.append(query)
+            query = query.astype(jnp.bfloat16)
+            scores.append([dot(query[:, part], reach[rows, part], ((1,), (1,))) for part in parts])
+        for c, query, score in zip(several, queries, scores):
+            rows = rows_of(c)
+            for part, one in zip(parts, score):
+                one = jnp.where(causal, one, 0.0).astype(jnp.bfloat16)
+                intra[rows, part] = dot(one, proj[VALUE, rows, part])
+            reach[rows, :] = (query * jnp.exp(centre[c])).astype(jnp.bfloat16)
 
     def chunk_loop(first, number):
         def step(i, carry):
-            chunk(first + i)
+            several = [first + 2 * i, first + 2 * i + 1]
+            state_part(several)
+            query_part(several)
             return carry
 
-        lax.fori_loop(0, number, step, 0)
+        lax.fori_loop(0, number // 2, step, 0)
 
     def mix(first, size):
         def step(i, carry):
@@ -176,8 +203,6 @@
 
     taps = taps_ref.shape[0]
     skip = REACH - taps + 1
-    pick = lax.broadcasted_iota(jnp.int32, (8, LANES), 0)
-    one_hot = [jnp.where(pick == k, 1.0, 0.0) for k in range(2)]
 
     def filter_tile(t):
         base = pl.multiple_of(t * LANES, LANES)
@@ -198,9 +223,8 @@
             value = filtered[pl.ds(base, LANES), lanes]
             sums = sums + value
             squares = squares + value * value
-        own_stats[:, pl.ds(base, LANES)] = exact(one_hot[0], sums, ((1,), (1,))) + exact(
-            one_hot[1], squares, ((1,), (1,))
-        )
+        own_stats[0:1, pl.ds(base, LANES)] = jnp.sum(sums.T, axis=0, keepdims=True)
+        own_stats[1:2, pl.ds(base, LANES)] = jnp.sum(squares.T, axis=0, keepdims=True)
 
     def filter_loop(first, number):
         def step(i, carry):
@@ -222,31 +246,29 @@
     chunk_loop(own_half // CHUNK, chip // CHUNK)
     pass_on(1)
     mix(own_half, chip)
-    filter_loop(own_half // LANES + 1, half_tiles - 1)
 
     def far_places(big):
         return [(0, cross * block + big * CHUNK, CHUNK), (CHUNK, diag * block + big * CHUNK, CHUNK)]
 
     def far_chunks(big):
-        def step(i, carry):
-            chunk(jnp.where(i == 0, cross, diag) * bigs + big)
-            return carry
-
-        lax.fori_loop(0, 2, step, 0)
+        return [owner * bigs + big for owner in (cross, diag)]
 
     for big in range(bigs):
         final = big == bigs - 1
+        if final:
+            filter_loop(own_half // LANES + 1, half_tiles - 1)
         for p in range(big * per, (big + 1) * per):
             if p > 1:
                 pass_on(p)
         for p in range(big * per, (big + 1) * per):
             handed[p].wait_recv()
         if final:
-            project(far_rows.at[big], 0, 3, far_places(big))
-            far_chunks(big)
+            project(far_rows.at[big], 0, 2, far_places(big))
         else:
             project(far_rows.at[big], 0, len(sources), far_places(big))
-            far_chunks(big)
+        state_part(far_chunks(big))
+        if not final:
+            query_part(far_chunks(big))
             for _, row, size in far_places(big):
                 mix(row, size)
 
@@ -269,13 +291,14 @@
         pack[h, head : head + PAD, :] = tail.astype(jnp.bfloat16)
         packs[h].start()
 
-    project(far_rows.at[bigs - 1], 3, len(sources), far_places(bigs - 1))
+    project(far_rows.at[bigs - 1], 2, len(sources), far_places(bigs - 1))
     for _, row, size in far_places(bigs - 1):
         mix(row, size)
     for g, lanes in enumerate(lanes_of):
         rim[0, :, lanes] = padded[g, rows_all : rows_all + REACH, :].astype(jnp.bfloat16)
     edge = remote(rim.at[0], rim.at[1], rim_sem.at[0], rim_sem.at[1], "sp", lax.rem(at + 1, count))
     edge.start()
+    query_part(far_chunks(bigs - 1))
 
     links = [
         remote(chain_out.at[h], chain_in.at[h], chain_send.at[h], chain_recv.at[h], "sp", lax.rem(at + 2, count))
@@ -341,7 +364,6 @@
         if relays:
             relays.pop(0)()
 
-    eye = jnp.where(pick == lax.broadcasted_iota(jnp.int32, (8, LANES), 1), 1.0, 0.0)
     for one in stats:
         one.wait_recv()
 
@@ -350,7 +372,10 @@
         total = own_stats[:, pl.ds(row, LANES)]
         for k in range(3):
             total = total + other_stats[k, :, pl.ds(row, LANES)]
-        moments[pl.ds(row, LANES), :] = exact(total, eye, ((0,), (0,)))
+        mean = total[0:1] / channels
+        scale = lax.rsqrt(total[1:2] / channels - mean * mean + norm_epsilon)
+        for k, value in enumerate((mean, scale)):
+            moments[k, pl.ds(row, LANES), :] = jnp.broadcast_to(value, (LANES, LANES)).T
         return carry
 
     lax.fori_loop(0, rows_all // LANES, stats_tile, 0)
@@ -364,8 +389,6 @@
             enter[c, h] = state.astype(jnp.bfloat16)
             if c < chunks - 1:
                 state = state * jnp.exp(closing[c, :, part]) + local[c, h]
-
-    channels = width * lax.axis_size("tp")
 
     def finish_rows(owner, low, size, slot):
         start = pl.multiple_of(owner * block + low, size)
@@ -377,11 +400,8 @@
             rec = rec * lax.rsqrt(jnp.mean(rec * rec, axis=-1, keepdims=True) + head_epsilon) * head_gain_ref[...]
             gate = proj[RGATE, rows, part].astype(jnp.float32)
             blend[target, part] = (rec * (gate * jax.nn.sigmoid(gate))).astype(jnp.bfloat16)
-        row_mean = moments[rows, 0:1] / channels
-        row_var = moments[rows, 1:2] / channels - row_mean * row_mean
-        scale = lax.rsqrt(row_var + norm_epsilon)
         for g, lanes in enumerate(lanes_of):
-            normed = (filtered[rows, lanes] - row_mean) * scale * conv_gain_ref[:, lanes]
+            normed = (filtered[rows, lanes] - moments[0, rows, :]) * moments[1, rows, :] * conv_gain_ref[:, lanes]
             blend[target, width + g * LANES : width + (g + 1) * LANES] = (normed * jax.nn.sigmoid(normed)).astype(
                 jnp.bfloat16
             )
@@ -414,6 +434,8 @@
         rows = pl.ds(p * turn, turn)
         finish_rows(diag, p * turn, turn, 0)
         finish_rows(cross, p * turn, turn, turn)
+        if p > 0:
+            settle(p - 1)
 
         def put(cols, result, p=p, rows=rows):
             to_pair[0, rows, cols] = result[0:turn].astype(jnp.bfloat16)
@@ -426,8 +448,6 @@
             )
         )
         lent[p].start()
-        if p > 0:
-            settle(p - 1)
     settle(RETURNS - 1)
     for big in range(bigs):
         rows = pl.ds(big * CHUNK, CHUNK)
@@ -487,10 +507,11 @@
     sems = lambda *shape: pltpu.SemaphoreType.DMA(shape)
     return pl.pallas_call(
         functools.partial(layer_kernel, head),
-        in_specs=[pl.BlockSpec(memory_space=pltpu.VMEM)] * 7 + [pl.BlockSpec(memory_space=pl.ANY)] * 8,
+        in_specs=[pl.BlockSpec(memory_space=pltpu.VMEM)] * 6 + [pl.BlockSpec(memory_space=pl.ANY)] * 9,
         out_specs=pl.BlockSpec(memory_space=pl.ANY),
         out_shape=jax.ShapeDtypeStruct((block, columns), bf16),
         scratch_shapes=[
+            vmem((block, depth), bf16),
             vmem((2, block, depth), bf16),
             vmem((block // CHUNK, 2 * CHUNK, depth), bf16),
             vmem((len(weights), depth, width), bf16),
@@ -499,6 +520,7 @@
             vmem((rows, width), f32),
             vmem((rows, width), bf16),
             vmem((chunks, heads, head, head), f32),
+            vmem((chunks, 1, width), f32),
             vmem((chunks, 1, width), f32),
             vmem((chunks, heads, head, head), bf16),
             vmem((heads, head, head), f32),
@@ -512,9 +534,9 @@
             vmem((2, REACH, width), bf16),
             vmem((groups, REACH + rows, LANES), f32),
             vmem((rows, width), f32),
-            vmem((8, rows), f32),
-            vmem((3, 8, rows), f32),
-            vmem((rows, LANES), f32),
+            vmem((2, rows), f32),
+            vmem((3, 2, rows), f32),
+            vmem((2, rows, LANES), f32),
             vmem((2 * CHUNK, 2 * width), bf16),
             vmem((2, turn, columns), f32),
             vmem((2, block, columns), bf16),
@@ -523,6 +545,7 @@
             vmem((block, columns), bf16),
             vmem((block, columns), f32),
             vmem((block, columns), bf16),
+            sems(SENDS),
             sems(len(weights) + 2),
             sems(3, SENDS),
             sems(3, SENDS),
@@ -541,8 +564,8 @@
             collective_id=0, has_side_effects=True, vmem_limit_bytes=65000 * 1024
         ),
     )(
-        tokens, norm_gain[None], forget_gap[None], decay_shift.T, conv_taps, conv_gain[None], head_gain[None],
-        *weights, out_rec, out_conv,
+        norm_gain[None], forget_gap[None], decay_shift.T, conv_taps, conv_gain[None], head_gain[None],
+        tokens, *weights, out_rec, out_conv,
     )
 
 

time: 89.5 us -> 81.4 us (0.909)
  Pallas kernels: 86.3 us -> 78.9 us
    pallas_call x1, Pallas kernels: 86.3 us -> 78.9 us  [on_device(): pl.pallas_call(functools.partial(layer_kernel, head), in_specs=[pl.BlockS...]
where the time goes in v2:
time: 81.4 us; the launch traced here: 81.2 us
  Pallas kernels  78.9 us (97%)
  local copies, waits for them, and re-layouts  2.3 us (3%)
    pallas_call x1, Pallas kernels, on_device(): pl.pallas_call(functools.partial(layer_kernel, head), in_specs=[pl.BlockS...  78.9 us
    unnamed x1, local copies, waits for them, and re-layouts  2.3 us

profile of v2, /device:TPU:25, one launch (start us, length us, event | category | flops | bytes accessed | tf_op | source)
XLA Modules:
  0.0 81.2 jit_solution(3957935206874816650)
XLA Ops:
  0.0 78.9 %shard_map.145 = bf16[256,2048]{1,0:T(8,128)(2,1)} custom-call(f32[1,2048]{1,0:T(1,128)} %bitcast.6, f32[1,512]{1,0:T(1,128)} %bitcast.7, f32[4,1024]{1,0:T(4,128)} %bitcast.5, f32[31,512]{1,0:T(8,128)} %taps_ref.1, f32[1,512]{1,0:T(1,128)} %bitcast.8, f32[1,128]{1,0:T(1,128)} %bitcast.9, bf16[256,2048]{1,0:T(8,128)(2,1)} %tokens_ref.1, ...), custom_call_target="tpu_custom_call" | custom-call | tf_op jit(solution)/shard_map/pallas_call | solution.py:508
  78.9 2.3 %copy.17 = bf16[256,2048]{1,0:T(8,128)(2,1)} copy(bf16[256,2048]{1,0:T(8,128)(2,1)} %shard_map.145) | data formatting | bytes 2097152

commit v3 on v2

--- a/solution.py
+++ b/solution.py
@@ -9,14 +9,14 @@
 
 CHUNK = 128
 PAD = 16
-SENDS = 4
+SENDS = 8
 RETURNS = 4
 REACH = 32
 TILE = 64
 LANES = 128
 SPAN = 512
 MESH = pl.DeviceIdType.MESH
-FORGET, VALUE, QUERY, GLU_VALUE, GLU_GATE, RGATE = range(6)
+FORGET, VALUE, GLU_VALUE, GLU_GATE, QUERY, RGATE = range(6)
 
 norm_epsilon = 1e-05
 head_epsilon = 1e-06
@@ -35,14 +35,15 @@
 
 
 def layer_kernel(
-    head, gain_ref, gap_ref, shift_ref, taps_ref, conv_gain_ref, head_gain_ref,
+    head, gain_in, gap_in, shift_in, taps_in, conv_gain_in, head_gain_in,
     tokens_ref, w0, w1, w2, w3, w4, w5, rec_rows, conv_rows, out_ref,
+    gain_ref, gap_ref, shift_ref, taps_ref, conv_gain_ref, head_gain_ref,
     raw, near_rows, far_rows, weight, merge, proj, intra, reach, local, closing, centre, enter,
     own_state, own_log, pack, pack_in, group_state, group_log, chain_out, chain_in,
     rim, padded, filtered, own_stats, other_stats, moments,
-    blend, held, to_pair, from_pair, to_cross, from_cross, mine, done,
-    raw_sem, weight_sem, send_sem, recv_sem, pack_send, pack_recv, chain_send, chain_recv,
-    rim_sem, stat_send, stat_recv, back_send, back_recv, out_sem,
+    blend, early, held, to_pair, from_pair, to_cross, from_cross, mine, done,
+    small_sem, raw_sem, weight_sem, send_sem, recv_sem, pack_send, pack_recv, chain_send, chain_recv,
+    rim_sem, stat_send, stat_recv, back_send, back_recv, first_send, first_recv, out_sem,
 ):
     block, depth = tokens_ref.shape
     piece = block // SENDS
@@ -51,6 +52,13 @@
         rows = pl.ds(p * piece, piece)
         raws.append(pltpu.make_async_copy(tokens_ref.at[rows, :], raw.at[rows, :], raw_sem.at[p]))
         raws[p].start()
+    smalls = []
+    for i, (far, near) in enumerate((
+        (gain_in, gain_ref), (gap_in, gap_ref), (shift_in, shift_ref), (taps_in, taps_ref),
+        (conv_gain_in, conv_gain_ref), (head_gain_in, head_gain_ref),
+    )):
+        smalls.append(pltpu.make_async_copy(far, near, small_sem.at[i]))
+        smalls[i].start()
     sources = (w0, w1, w2, w3, w4, w5)
     width = gap_ref.shape[1]
     fetched = [pltpu.make_async_copy(w, weight.at[i], weight_sem.at[i]) for i, w in enumerate(sources)]
@@ -67,9 +75,18 @@
     barrier = pltpu.get_barrier_semaphore()
     for other in (pair, cross, diag):
         pl.semaphore_signal(barrier, inc=1, device_id={"tp": other}, device_id_type=MESH)
-    for hop in (1, 2, count - 1, count - 2):
-        pl.semaphore_signal(barrier, inc=1, device_id={"sp": lax.rem(at + hop, count)}, device_id_type=MESH)
-    pl.semaphore_wait(barrier, 7)
+    pl.semaphore_signal(barrier, inc=1, device_id={"sp": mate}, device_id_type=MESH)
+
+    @pl.when(team > 0)
+    def _():
+        pl.semaphore_signal(barrier, inc=1, device_id={"sp": at - 2}, device_id_type=MESH)
+
+    @pl.when((team > 0) & (side == 0))
+    def _():
+        pl.semaphore_signal(barrier, inc=1, device_id={"sp": at - 1}, device_id_type=MESH)
+
+    onward = team < teams - 1
+    pl.semaphore_wait(barrier, jnp.where(onward, jnp.where(side == 1, 6, 5), 4))
 
     rows_all = proj.shape[1]
     heads, chunks = width // head, rows_all // CHUNK
@@ -84,7 +101,7 @@
             device_id={axis: device}, device_id_type=MESH,
         )
 
-    for one in raws:
+    for one in raws + smalls:
         one.wait()
     for one in fetched:
         one.start()
@@ -204,11 +221,9 @@
     taps = taps_ref.shape[0]
     skip = REACH - taps + 1
 
-    def filter_tile(t):
-        base = pl.multiple_of(t * LANES, LANES)
-
+    def filter_rows(row0, number):
         def step(i, carry):
-            g, row = i // (LANES // TILE), base + lax.rem(i, LANES // TILE) * TILE
+            g, row = i // number, row0 + lax.rem(i, number) * TILE
             lanes = pl.ds(pl.multiple_of(g * LANES, LANES), LANES)
             total = jnp.zeros((TILE, LANES), jnp.float32)
             for j in range(taps):
@@ -216,7 +231,11 @@
             filtered[pl.ds(pl.multiple_of(row, TILE), TILE), lanes] = total
             return carry
 
-        lax.fori_loop(0, len(lanes_of) * (LANES // TILE), step, 0)
+        lax.fori_loop(0, len(lanes_of) * number, step, 0)
+
+    def filter_tile(t, low=0):
+        base = pl.multiple_of(t * LANES, LANES)
+        filter_rows(base, (LANES - low) // TILE)
         sums = jnp.zeros((LANES, LANES), jnp.float32)
         squares = jnp.zeros((LANES, LANES), jnp.float32)
         for lanes in lanes_of:
@@ -244,8 +263,11 @@
     project(near_rows.at[1], 0, len(sources), [(0, pair * block, block)])
     pass_on(0)
     chunk_loop(own_half // CHUNK, chip // CHUNK)
-    pass_on(1)
+    for p in range(1, per - 1):
+        pass_on(p)
     mix(own_half, chip)
+    filter_loop(own_half // LANES + 1, half_tiles - 2)
+    pass_on(per - 1)
 
     def far_places(big):
         return [(0, cross * block + big * CHUNK, CHUNK), (CHUNK, diag * block + big * CHUNK, CHUNK)]
@@ -253,27 +275,38 @@
     def far_chunks(big):
         return [owner * bigs + big for owner in (cross, diag)]
 
-    for big in range(bigs):
-        final = big == bigs - 1
-        if final:
-            filter_loop(own_half // LANES + 1, half_tiles - 1)
-        for p in range(big * per, (big + 1) * per):
-            if p > 1:
-                pass_on(p)
-        for p in range(big * per, (big + 1) * per):
+    far_tile = far_half // LANES
+    for big in range(bigs - 1):
+        begin = big * per
+        for p in range(begin, begin + per):
             handed[p].wait_recv()
-        if final:
-            project(far_rows.at[big], 0, 2, far_places(big))
-        else:
-            project(far_rows.at[big], 0, len(sources), far_places(big))
+        project(far_rows.at[big], 0, len(sources), far_places(big))
+        pass_on(begin + per)
         state_part(far_chunks(big))
-        if not final:
-            query_part(far_chunks(big))
-            for _, row, size in far_places(big):
-                mix(row, size)
+        query_part(far_chunks(big))
+        for _, row, size in far_places(big):
+            mix(row, size)
+        for p in range(begin + per + 1, begin + 2 * per - 2):
+            pass_on(p)
+        if big == bigs - 2:
+            filter_tile(own_half // LANES + half_tiles - 1)
+            for tile in (own_half // LANES, far_tile, far_tile + bigs):
+                filter_rows(pl.multiple_of(tile * LANES + TILE, TILE), 1)
+        for p in range(begin + 2 * per - 2, begin + 2 * per):
+            pass_on(p)
+    for p in range(SENDS - per, SENDS):
+        handed[p].wait_recv()
+    project(far_rows.at[bigs - 1], 0, 2, far_places(bigs - 1))
+    state_part(far_chunks(bigs - 1))
 
     place = lax.broadcasted_iota(jnp.int32, (PAD, head), 0)
-    packs = [remote(pack.at[h], pack_in.at[h], pack_send.at[h], pack_recv.at[h], "sp", mate) for h in range(heads)]
+    half = head // 2
+    units = [(h, k) for h in range(heads) for k in range(2)]
+    spans = (pl.ds(0, PAD + half), pl.ds(PAD + half, half))
+    packs = [
+        remote(pack.at[h, spans[k], :], pack_in.at[h, spans[k], :], pack_send.at[h, k], pack_recv.at[h, k], "sp", mate)
+        for h, k in units
+    ]
     for h in range(heads):
         part = slice(h * head, (h + 1) * head)
         state, log = local[0, h], closing[0, :, part]
@@ -282,92 +315,102 @@
             log = log + closing[c, :, part]
         own_state[h] = state
         own_log[:, part] = log
-        pack[h, 0:head, :] = state.astype(jnp.bfloat16)
+        pack[h, PAD : PAD + head, :] = state.astype(jnp.bfloat16)
         high = log.astype(jnp.bfloat16).astype(jnp.float32)
         rest = log - high
         mid = rest.astype(jnp.bfloat16).astype(jnp.float32)
         low = rest - mid
         tail = jnp.where(place == 0, high, jnp.where(place == 1, mid, jnp.where(place == 2, low, 0.0)))
-        pack[h, head : head + PAD, :] = tail.astype(jnp.bfloat16)
-        packs[h].start()
-
-    project(far_rows.at[bigs - 1], 2, len(sources), far_places(bigs - 1))
+        pack[h, 0:PAD, :] = tail.astype(jnp.bfloat16)
+        packs[2 * h].start()
+        packs[2 * h + 1].start()
+
+    project(far_rows.at[bigs - 1], 2, 4, far_places(bigs - 1))
     for _, row, size in far_places(bigs - 1):
         mix(row, size)
     for g, lanes in enumerate(lanes_of):
         rim[0, :, lanes] = padded[g, rows_all : rows_all + REACH, :].astype(jnp.bfloat16)
     edge = remote(rim.at[0], rim.at[1], rim_sem.at[0], rim_sem.at[1], "sp", lax.rem(at + 1, count))
-    edge.start()
-    query_part(far_chunks(bigs - 1))
+    ahead = onward | (side == 0)
+    pl.when(ahead)(edge.start)
 
     links = [
-        remote(chain_out.at[h], chain_in.at[h], chain_send.at[h], chain_recv.at[h], "sp", lax.rem(at + 2, count))
-        for h in range(heads)
+        remote(
+            chain_out.at[h, pl.ds(k * half, half), :], chain_in.at[h, pl.ds(k * half, half), :],
+            chain_send.at[h, k], chain_recv.at[h, k], "sp", lax.rem(at + 2, count),
+        )
+        for h, k in units
     ]
 
     def mate_log(h):
-        tail = pack_in[h, head : head + PAD, :].astype(jnp.float32)
+        tail = pack_in[h, 0:PAD, :].astype(jnp.float32)
         return tail[0:1] + tail[1:2] + tail[2:3]
 
-    for h in range(heads):
-        part = slice(h * head, (h + 1) * head)
-        packs[h].wait_recv()
-        theirs, log = pack_in[h, 0:head, :].astype(jnp.float32), mate_log(h)
-        ours, own = own_state[h], own_log[:, part]
+    def meet(u):
+        h, k = units[u]
+        some = pl.ds(k * half, half)
+        packs[u].wait_recv()
+        theirs, log = pack_in[h, PAD + k * half : PAD + (k + 1) * half, :].astype(jnp.float32), mate_log(h)
+        ours, own = own_state[h, some, :], own_log[:, parts[h]]
         first = jnp.where(side == 0, ours, theirs)
         second = jnp.where(side == 0, theirs, ours)
-        group_state[h] = first * jnp.exp(jnp.where(side == 0, log, own)) + second
-        group_log[:, part] = log + own
+        group = first * jnp.exp(jnp.where(side == 0, log, own)) + second
+        group_state[h, some, :] = group
+        if k == 0:
+            group_log[:, parts[h]] = log + own
 
         @pl.when(team == 0)
         def _():
-            chain_in[h] = jnp.zeros((head, head), jnp.bfloat16)
-            chain_out[h] = group_state[h].astype(jnp.bfloat16)
-            links[h].start()
-
-    def relay(k):
+            chain_in[h, some, :] = jnp.zeros((half, head), jnp.bfloat16)
+            chain_out[h, some, :] = group.astype(jnp.bfloat16)
+            links[u].start()
+
+    def relay(k, first, last):
         @pl.when(team == k)
         def _():
-            for h in range(heads):
-                links[h].wait_recv()
+            for u in range(first, last):
+                h, some = units[u][0], pl.ds(units[u][1] * half, half)
+                links[u].wait_recv()
                 if k < teams - 1:
-                    part = slice(h * head, (h + 1) * head)
-                    step = chain_in[h].astype(jnp.float32) * jnp.exp(group_log[:, part]) + group_state[h]
-                    chain_out[h] = step.astype(jnp.bfloat16)
-                    links[h].start()
-
-    far_tile = far_half // LANES
+                    step = chain_in[h, some, :].astype(jnp.float32) * jnp.exp(group_log[:, parts[h]])
+                    chain_out[h, some, :] = (step + group_state[h, some, :]).astype(jnp.bfloat16)
+                    links[u].start()
 
     def rim_in():
-        edge.wait_recv()
+        pl.when(at > 0)(edge.wait_recv)
         for g, lanes in enumerate(lanes_of):
             padded[g, 0:REACH, :] = jnp.where(at > 0, rim[1, :, lanes].astype(jnp.float32), 0.0)
-        filter_tile(own_half // LANES)
 
     stats = [
         remote(own_stats, other_stats.at[k - 1], stat_send.at[k - 1], stat_recv.at[k - 1], "tp", lax.rem(me + k, 4))
         for k in range(1, 4)
     ]
-
-    def send_stats():
-        filter_tile(far_tile)
-        for one in stats:
-            one.start()
-
-    work = [lambda: filter_loop(far_tile + 1, 2), lambda: filter_loop(far_tile + 3, 1), rim_in, send_stats]
-    if half_tiles != 4:
-        work[1] = lambda: filter_loop(far_tile + 3, half_tiles - 3)
-    relays = [functools.partial(relay, k) for k in range(1, teams)]
-    while work or relays:
-        if work:
-            work.pop(0)()
-        if relays:
-            relays.pop(0)()
-
+    number = len(units)
+    for u in range(0, 3):
+        meet(u)
+    filter_tile(far_tile + 1)
+    for u in range(3, 6):
+        meet(u)
+    filter_tile(far_tile + bigs, TILE)
+    for u in range(6, number):
+        meet(u)
+    relay(1, 0, 3)
+    if bigs > 2:
+        filter_loop(far_tile + 2, bigs - 2)
+    filter_loop(far_tile + bigs + 1, bigs - 1)
+    relay(1, 3, 6)
+    rim_in()
+    filter_tile(own_half // LANES, TILE)
+    relay(1, 6, number)
+    filter_tile(far_tile, TILE)
+    for one in stats:
+        one.start()
+    if teams > 3:
+        relay(2, 0, number)
     for one in stats:
         one.wait_recv()
 
-    def stats_tile(i, carry):
+    def stats_tile(i):
         row = pl.multiple_of(i * LANES, LANES)
         total = own_stats[:, pl.ds(row, LANES)]
         for k in range(3):
@@ -376,65 +419,117 @@
         scale = lax.rsqrt(total[1:2] / channels - mean * mean + norm_epsilon)
         for k, value in enumerate((mean, scale)):
             moments[k, pl.ds(row, LANES), :] = jnp.broadcast_to(value, (LANES, LANES)).T
-        return carry
-
-    lax.fori_loop(0, rows_all // LANES, stats_tile, 0)
+
+    for owner in (diag, cross):
+        stats_tile(owner * bigs)
+
+    def conv_part(owner, low, size, slot):
+        rows, target = pl.ds(pl.multiple_of(owner * block + low, size), size), pl.ds(slot, size)
+        for g, lanes in enumerate(lanes_of):
+            normed = (filtered[rows, lanes] - moments[0, rows, :]) * moments[1, rows, :] * conv_gain_ref[:, lanes]
+            blend[target, width + g * LANES : width + (g + 1) * LANES] = (normed * jax.nn.sigmoid(normed)).astype(
+                jnp.bfloat16
+            )
+
+    columns = merge.shape[1]
+    turn = block // RETURNS
+
+    def spread(size, put, first=0, last=2 * width):
+        def step(j, carry):
+            cols = pl.ds(pl.multiple_of(j * SPAN, SPAN), SPAN)
+            put(cols, dot(blend[0:size, first:last], merge[first:last, cols]))
+            return carry
+
+        lax.fori_loop(0, columns // SPAN, step, 0)
+
+    for one in fetched[len(sources) :]:
+        one.wait()
+    conv_part(diag, 0, turn, 0)
+    conv_part(cross, 0, turn, turn)
+
+    def put_early(cols, result):
+        early[:, cols] = result
+
+    spread(2 * turn, put_early, first=width)
+    for k in range(3 if teams > 3 else 2, teams):
+        relay(k, 0, number)
 
     for h in range(heads):
         part = slice(h * head, (h + 1) * head)
         state = chain_in[h].astype(jnp.float32)
-        moved = state * jnp.exp(mate_log(h)) + pack_in[h, 0:head, :].astype(jnp.float32)
+        moved = state * jnp.exp(mate_log(h)) + pack_in[h, PAD : PAD + head, :].astype(jnp.float32)
         state = jnp.where(side == 1, moved, state)
         for c in range(chunks):
             enter[c, h] = state.astype(jnp.bfloat16)
             if c < chunks - 1:
                 state = state * jnp.exp(closing[c, :, part]) + local[c, h]
 
-    def finish_rows(owner, low, size, slot):
-        start = pl.multiple_of(owner * block + low, size)
-        rows, c = pl.ds(start, size), owner * bigs + low // CHUNK
-        target = pl.ds(slot, size)
-        for h in range(heads):
-            part = slice(h * head, (h + 1) * head)
+    def rec_part(owner, low, size, slot):
+        rows, target = pl.ds(pl.multiple_of(owner * block + low, size), size), pl.ds(slot, size)
+        c = owner * bigs + low // CHUNK
+        for h, part in enumerate(parts):
             rec = intra[rows, part] + dot(reach[rows, part], enter[c, h], ((1,), (1,)))
             rec = rec * lax.rsqrt(jnp.mean(rec * rec, axis=-1, keepdims=True) + head_epsilon) * head_gain_ref[...]
             gate = proj[RGATE, rows, part].astype(jnp.float32)
             blend[target, part] = (rec * (gate * jax.nn.sigmoid(gate))).astype(jnp.bfloat16)
-        for g, lanes in enumerate(lanes_of):
-            normed = (filtered[rows, lanes] - moments[0, rows, :]) * moments[1, rows, :] * conv_gain_ref[:, lanes]
-            blend[target, width + g * LANES : width + (g + 1) * LANES] = (normed * jax.nn.sigmoid(normed)).astype(
-                jnp.bfloat16
-            )
-
-    columns = merge.shape[1]
-
-    def spread(size, put):
-        def step(j, carry):
-            cols = pl.ds(pl.multiple_of(j * SPAN, SPAN), SPAN)
-            put(cols, dot(blend[0:size, :], merge[:, cols]))
-            return carry
-
-        lax.fori_loop(0, columns // SPAN, step, 0)
-
-    for one in fetched[len(sources) :]:
-        one.wait()
-    turn = block // RETURNS
-    lent, returned, close = [], [], []
+
+    def finish_rows(owner, low, size, slot):
+        rec_part(owner, low, size, slot)
+        conv_part(owner, low, size, slot)
+
+    lent, returned, close = {}, {}, []
 
     def settle(p):
         rows = pl.ds(p * turn, turn)
         lent[p].wait_recv()
         to_cross[rows, :] = (held[p % 2] + from_pair[0, rows, :].astype(jnp.float32)).astype(jnp.bfloat16)
-        returned.append(
-            remote(to_cross.at[rows, :], from_cross.at[rows, :], back_send.at[1, p], back_recv.at[1, p], "tp", cross)
+        returned[p] = remote(
+            to_cross.at[rows, :], from_cross.at[rows, :], back_send.at[1, p], back_recv.at[1, p], "tp", cross
         )
         returned[p].start()
 
-    for p in range(RETURNS):
+    late = (bigs - 1) * CHUNK // turn
+    head_rows = pl.ds(0, turn)
+    first_lent, first_returned = [], []
+    rec_part(diag, 0, turn, 0)
+    rec_part(cross, 0, turn, turn)
+    for j in range(columns // SPAN):
+        cols = slice(j * SPAN, (j + 1) * SPAN)
+        result = dot(blend[0 : 2 * turn, 0:width], merge[0:width, cols]) + early[:, cols]
+        to_pair[0, head_rows, cols] = result[0:turn].astype(jnp.bfloat16)
+        held[0, :, cols] = result[turn : 2 * turn]
+        first_lent.append(
+            remote(
+                to_pair.at[0, head_rows, cols], from_pair.at[0, head_rows, cols],
+                first_send.at[0, j], first_recv.at[0, j], "tp", pair,
+            )
+        )
+        first_lent[j].start()
+    for j in range(columns // SPAN):
+        cols = slice(j * SPAN, (j + 1) * SPAN)
+        first_lent[j].wait_recv()
+        to_cross[head_rows, cols] = (held[0, :, cols] + from_pair[0, head_rows, cols].astype(jnp.float32)).astype(
+            jnp.bfloat16
+        )
+        first_returned.append(
+            remote(
+                to_cross.at[head_rows, cols], from_cross.at[head_rows, cols],
+                first_send.at[1, j], first_recv.at[1, j], "tp", cross,
+            )
+        )
+        first_returned[j].start()
+    for p in range(1, RETURNS):
         rows = pl.ds(p * turn, turn)
+        if p == late:
+            settle(p - 1)
+            project(far_rows.at[bigs - 1], 4, len(sources), far_places(bigs - 1))
+            query_part(far_chunks(bigs - 1))
+            for owner in (diag, cross):
+                for big in range(1, bigs):
+                    stats_tile(owner * bigs + big)
         finish_rows(diag, p * turn, turn, 0)
         finish_rows(cross, p * turn, turn, turn)
-        if p > 0:
+        if p > 1 and p != late:
             settle(p - 1)
 
         def put(cols, result, p=p, rows=rows):
@@ -442,13 +537,14 @@
             held[p % 2, :, cols] = result[turn : 2 * turn]
 
         spread(2 * turn, put)
-        lent.append(
-            remote(
-                to_pair.at[0, rows, :], from_pair.at[0, rows, :], back_send.at[0, p], back_recv.at[0, p], "tp", pair
-            )
+        lent[p] = remote(
+            to_pair.at[0, rows, :], from_pair.at[0, rows, :], back_send.at[0, p], back_recv.at[0, p], "tp", pair
         )
         lent[p].start()
     settle(RETURNS - 1)
+    for owner in (pair, me):
+        for big in range(bigs):
+            stats_tile(owner * bigs + big)
     for big in range(bigs):
         rows = pl.ds(big * CHUNK, CHUNK)
         finish_rows(pair, big * CHUNK, CHUNK, 0)
@@ -473,14 +569,20 @@
     stores = []
     for p in range(RETURNS):
         rows = pl.ds(p * turn, turn)
-        returned[p].wait_recv()
+        for one in first_returned if p == 0 else [returned[p]]:
+            one.wait_recv()
         done[rows, :] = (mine[rows, :] + from_cross[rows, :].astype(jnp.float32)).astype(jnp.bfloat16)
         stores.append(pltpu.make_async_copy(done.at[rows, :], out_ref.at[rows, :], out_sem.at[p]))
         stores[p].start()
-    for one in crossing + nearby + handed + packs + [edge] + stats + lent + returned + close:
+    for one in crossing + nearby + handed + packs + stats + first_lent + first_returned + close:
         one.wait_send()
-
-    @pl.when(team < teams - 1)
+    for p in range(1, RETURNS):
+        lent[p].wait_send()
+        returned[p].wait_send()
+
+    pl.when(ahead)(edge.wait_send)
+
+    @pl.when(onward)
     def _():
         for one in links:
             one.wait_send()
@@ -493,7 +595,7 @@
     tokens, norm_gain, w_query, w_forget, w_value, w_rgate, w_glu_value, w_glu_gate, forget_gap,
     decay_shift, head_gain, conv_taps, conv_gain, out_rec, out_conv,
 ):
-    weights = (w_forget, w_value, w_query, w_glu_value, w_glu_gate, w_rgate)
+    weights = (w_forget, w_value, w_glu_value, w_glu_gate, w_query, w_rgate)
     block, depth = tokens.shape
     width, columns = out_rec.shape
     head = head_gain.shape[0]
@@ -507,10 +609,16 @@
     sems = lambda *shape: pltpu.SemaphoreType.DMA(shape)
     return pl.pallas_call(
         functools.partial(layer_kernel, head),
-        in_specs=[pl.BlockSpec(memory_space=pltpu.VMEM)] * 6 + [pl.BlockSpec(memory_space=pl.ANY)] * 9,
+        in_specs=[pl.BlockSpec(memory_space=pl.ANY)] * 15,
         out_specs=pl.BlockSpec(memory_space=pl.ANY),
         out_shape=jax.ShapeDtypeStruct((block, columns), bf16),
         scratch_shapes=[
+            vmem((1, depth), f32),
+            vmem((1, width), f32),
+            vmem((heads, rows), f32),
+            vmem(conv_taps.shape, f32),
+            vmem((1, width), f32),
+            vmem((1, head), f32),
             vmem((block, depth), bf16),
             vmem((2, block, depth), bf16),
             vmem((block // CHUNK, 2 * CHUNK, depth), bf16),
@@ -538,6 +646,7 @@
             vmem((3, 2, rows), f32),
             vmem((2, rows, LANES), f32),
             vmem((2 * CHUNK, 2 * width), bf16),
+            vmem((2 * turn, columns), f32),
             vmem((2, turn, columns), f32),
             vmem((2, block, columns), bf16),
             vmem((2, block, columns), bf16),
@@ -545,19 +654,22 @@
             vmem((block, columns), bf16),
             vmem((block, columns), f32),
             vmem((block, columns), bf16),
+            sems(6),
             sems(SENDS),
             sems(len(weights) + 2),
             sems(3, SENDS),
             sems(3, SENDS),
-            sems(heads),
-            sems(heads),
-            sems(heads),
-            sems(heads),
+            sems(heads, 2),
+            sems(heads, 2),
+            sems(heads, 2),
+            sems(heads, 2),
             sems(2),
             sems(3),
             sems(3),
             sems(3, RETURNS),
             sems(3, RETURNS),
+            sems(2, columns // SPAN),
+            sems(2, columns // SPAN),
             sems(RETURNS),
         ],
         compiler_params=pltpu.CompilerParams(

time: 81.4 us -> 73 us (0.90)
  Pallas kernels: 78.9 us -> 70.6 us
    pallas_call x1, Pallas kernels: 78.9 us -> 70.6 us  [on_device(): pl.pallas_call(functools.partial(layer_kernel, head), in_specs=[pl.BlockS...]
where the time goes in v3:
time: 73 us; the launch traced here: 72.9 us
  Pallas kernels  70.6 us (97%)
  local copies, waits for them, and re-layouts  2.3 us (3%)
    pallas_call x1, Pallas kernels, on_device(): pl.pallas_call(functools.partial(layer_kernel, head), in_specs=[pl.BlockS...  70.6 us
    unnamed x1, local copies, waits for them, and re-layouts  2.3 us

profile of v3, /device:TPU:25, one launch (start us, length us, event | category | flops | bytes accessed | tf_op | source)
XLA Modules:
  0.0 72.9 jit_solution(8808326347405149844)
XLA Ops:
  0.0 70.6 %shard_map.145 = bf16[256,2048]{1,0:T(8,128)(2,1)} custom-call(f32[1,2048]{1,0:T(1,128)} %bitcast.6, f32[1,512]{1,0:T(1,128)} %bitcast.7, f32[4,1024]{1,0:T(4,128)} %bitcast.5, f32[31,512]{1,0:T(8,128)} %taps_in.1, f32[1,512]{1,0:T(1,128)} %bitcast.8, f32[1,128]{1,0:T(1,128)} %bitcast.9, bf16[256,2048]{1,0:T(8,128)(2,1)} %tokens_ref.1, ...), custom_call_target="tpu_custom_call" | custom-call | tf_op jit(solution)/shard_map/pallas_call | solution.py:610
  70.6 2.3 %copy.17 = bf16[256,2048]{1,0:T(8,128)(2,1)} copy(bf16[256,2048]{1,0:T(8,128)(2,1)} %shard_map.145) | data formatting | bytes 2097152

commit v4 on v3

--- a/solution.py
+++ b/solution.py
@@ -41,17 +41,16 @@
     raw, near_rows, far_rows, weight, merge, proj, intra, reach, local, closing, centre, enter,
     own_state, own_log, pack, pack_in, group_state, group_log, chain_out, chain_in,
     rim, padded, filtered, own_stats, other_stats, moments,
-    blend, early, held, to_pair, from_pair, to_cross, from_cross, mine, done,
-    small_sem, raw_sem, weight_sem, send_sem, recv_sem, pack_send, pack_recv, chain_send, chain_recv,
-    rim_sem, stat_send, stat_recv, back_send, back_recv, first_send, first_recv, out_sem,
+    blend, early, held, to_pair, from_pair, to_cross, from_cross, mine,
+    small_sem, raw_sem, weight_sem, send_sem, cross_sem, near_sem, hand_sem, pack_send, pack_recv, chain_send, chain_recv,
+    rim_sem, stat_send, stat_recv, back_send, lent_sem, back_sem, close_sem, first_send, first_recv, first_done,
 ):
     block, depth = tokens_ref.shape
     piece = block // SENDS
     raws = []
-    for p in range(SENDS):
-        rows = pl.ds(p * piece, piece)
-        raws.append(pltpu.make_async_copy(tokens_ref.at[rows, :], raw.at[rows, :], raw_sem.at[p]))
-        raws[p].start()
+    for i, rows in enumerate((pl.ds(0, piece), pl.ds(piece, block - piece))):
+        raws.append(pltpu.make_async_copy(tokens_ref.at[rows, :], raw.at[rows, :], raw_sem.at[i]))
+        raws[i].start()
     smalls = []
     for i, (far, near) in enumerate((
         (gain_in, gain_ref), (gap_in, gap_ref), (shift_in, shift_ref), (taps_in, taps_ref),
@@ -101,31 +100,35 @@
             device_id={axis: device}, device_id_type=MESH,
         )
 
-    for one in raws + smalls:
-        one.wait()
-    for one in fetched:
-        one.start()
+    smalls[0].wait()
 
     crossing, nearby, handed = [], [], []
     for p in range(SENDS):
         rows = pl.ds(p * piece, piece)
+        if p < 2:
+            raws[p].wait()
+        if p == 1:
+            for one in fetched:
+                one.start()
         near_rows[0, rows, :] = layer_norm(raw[rows, :], gain_ref[...]).astype(jnp.bfloat16)
         big, low = p // per, (p % per) * piece
         landing = far_rows.at[big, pl.ds(low, piece), :]
-        crossing.append(remote(near_rows.at[0, rows, :], landing, send_sem.at[0, p], recv_sem.at[0, p], "tp", cross))
+        crossing.append(remote(near_rows.at[0, rows, :], landing, send_sem.at[0], cross_sem.at[p], "tp", cross))
         nearby.append(
             remote(
-                near_rows.at[0, rows, :], near_rows.at[1, rows, :], send_sem.at[1, p], recv_sem.at[1, p], "tp", pair
+                near_rows.at[0, rows, :], near_rows.at[1, rows, :], send_sem.at[1], near_sem.at[0], "tp", pair
             )
         )
         handed.append(
             remote(
                 landing, far_rows.at[big, pl.ds(CHUNK + low, piece), :],
-                send_sem.at[2, p], recv_sem.at[2, p], "tp", pair,
+                send_sem.at[2], hand_sem.at[big], "tp", pair,
             )
         )
         crossing[p].start()
         nearby[p].start()
+    for one in smalls[1:]:
+        one.wait()
 
     def project(values, first, last, places, ready=False):
         def step(k, carry):
@@ -145,6 +148,10 @@
         crossing[p].wait_recv()
         handed[p].start()
 
+    def handed_in(big):
+        part = far_rows.at[big, pl.ds(CHUNK, CHUNK), :]
+        remote(part, part, send_sem.at[2], hand_sem.at[big], "tp", pair).wait_recv()
+
     row_at = lax.broadcasted_iota(jnp.int32, (CHUNK, CHUNK), 0)
     col_at = lax.broadcasted_iota(jnp.int32, (CHUNK, CHUNK), 1)
     causal = row_at >= col_at
@@ -156,12 +163,14 @@
     def rows_of(c):
         return pl.ds(pl.multiple_of(c * CHUNK, CHUNK), CHUNK)
 
-    def state_part(several):
+    def state_part(several, group=None):
+        group = list(range(heads)) if group is None else group
+        wide = slice(group[0] * head, (group[-1] + 1) * head)
         keys, totals = [], []
         for c in several:
             rows = rows_of(c)
-            key = gap_ref[...] * jax.nn.sigmoid(-proj[FORGET, rows, :].astype(jnp.float32))
-            shift = [jnp.broadcast_to(shift_ref[h : h + 1, rows], (head, CHUNK)).T for h in range(heads)]
+            key = gap_ref[:, wide] * jax.nn.sigmoid(-proj[FORGET, rows, wide].astype(jnp.float32))
+            shift = [jnp.broadcast_to(shift_ref[h : h + 1, rows], (head, CHUNK)).T for h in group]
             log = jnp.log1p(-key) + jnp.concatenate(shift, axis=1)
             high = log.astype(jnp.bfloat16)
             low = (log - high.astype(jnp.float32)).astype(jnp.bfloat16)
@@ -173,13 +182,13 @@
             middle = total[CHUNK // 2 - 1 : CHUNK // 2, :]
             total = total - middle
             key_mid = key * jnp.exp(-total)
-            intra[rows, :] = total
-            reach[rows, :] = key_mid.astype(jnp.bfloat16)
+            intra[rows, wide] = total
+            reach[rows, wide] = key_mid.astype(jnp.bfloat16)
             key_end = (key_mid * jnp.exp(last - middle)).astype(jnp.bfloat16)
-            for h, part in enumerate(parts):
-                local[c, h] = dot(proj[VALUE, rows, part], key_end[:, part], ((0,), (0,)))
-            closing[c] = last
-            centre[c] = middle
+            for i, h in enumerate(group):
+                local[c, h] = dot(proj[VALUE, rows, parts[h]], key_end[:, parts[i]], ((0,), (0,)))
+            closing[c, :, wide] = last
+            centre[c, :, wide] = middle
 
     def query_part(several):
         queries, scores = [], []
@@ -233,9 +242,8 @@
 
         lax.fori_loop(0, len(lanes_of) * number, step, 0)
 
-    def filter_tile(t, low=0):
+    def tally(t):
         base = pl.multiple_of(t * LANES, LANES)
-        filter_rows(base, (LANES - low) // TILE)
         sums = jnp.zeros((LANES, LANES), jnp.float32)
         squares = jnp.zeros((LANES, LANES), jnp.float32)
         for lanes in lanes_of:
@@ -245,6 +253,10 @@
         own_stats[0:1, pl.ds(base, LANES)] = jnp.sum(sums.T, axis=0, keepdims=True)
         own_stats[1:2, pl.ds(base, LANES)] = jnp.sum(squares.T, axis=0, keepdims=True)
 
+    def filter_tile(t):
+        filter_rows(pl.multiple_of(t * LANES, LANES), LANES // TILE)
+        tally(t)
+
     def filter_loop(first, number):
         def step(i, carry):
             filter_tile(first + i)
@@ -258,8 +270,7 @@
     half_tiles = chip // LANES
 
     project(near_rows.at[0], 0, len(sources), [(0, me * block, block)], ready=True)
-    for one in nearby:
-        one.wait_recv()
+    remote(near_rows.at[0], near_rows.at[1], send_sem.at[1], near_sem.at[0], "tp", pair).wait_recv()
     project(near_rows.at[1], 0, len(sources), [(0, pair * block, block)])
     pass_on(0)
     chunk_loop(own_half // CHUNK, chip // CHUNK)
@@ -278,8 +289,7 @@
     far_tile = far_half // LANES
     for big in range(bigs - 1):
         begin = big * per
-        for p in range(begin, begin + per):
-            handed[p].wait_recv()
+        handed_in(big)
         project(far_rows.at[big], 0, len(sources), far_places(big))
         pass_on(begin + per)
         state_part(far_chunks(big))
@@ -294,20 +304,18 @@
                 filter_rows(pl.multiple_of(tile * LANES + TILE, TILE), 1)
         for p in range(begin + 2 * per - 2, begin + 2 * per):
             pass_on(p)
-    for p in range(SENDS - per, SENDS):
-        handed[p].wait_recv()
+    handed_in(bigs - 1)
     project(far_rows.at[bigs - 1], 0, 2, far_places(bigs - 1))
-    state_part(far_chunks(bigs - 1))
 
     place = lax.broadcasted_iota(jnp.int32, (PAD, head), 0)
     half = head // 2
     units = [(h, k) for h in range(heads) for k in range(2)]
     spans = (pl.ds(0, PAD + half), pl.ds(PAD + half, half))
     packs = [
-        remote(pack.at[h, spans[k], :], pack_in.at[h, spans[k], :], pack_send.at[h, k], pack_recv.at[h, k], "sp", mate)
+        remote(pack.at[h, spans[k], :], pack_in.at[h, spans[k], :], pack_send.at[0], pack_recv.at[h, k], "sp", mate)
         for h, k in units
     ]
-    for h in range(heads):
+    def send_state(h):
         part = slice(h * head, (h + 1) * head)
         state, log = local[0, h], closing[0, :, part]
         for c in range(1, chunks):
@@ -325,6 +333,9 @@
         packs[2 * h].start()
         packs[2 * h + 1].start()
 
+    state_part(far_chunks(bigs - 1))
+    for h in range(heads):
+        send_state(h)
     project(far_rows.at[bigs - 1], 2, 4, far_places(bigs - 1))
     for _, row, size in far_places(bigs - 1):
         mix(row, size)
@@ -337,7 +348,7 @@
     links = [
         remote(
             chain_out.at[h, pl.ds(k * half, half), :], chain_in.at[h, pl.ds(k * half, half), :],
-            chain_send.at[h, k], chain_recv.at[h, k], "sp", lax.rem(at + 2, count),
+            chain_send.at[0], chain_recv.at[h, k], "sp", lax.rem(at + 2, count),
         )
         for h, k in units
     ]
@@ -382,33 +393,43 @@
             padded[g, 0:REACH, :] = jnp.where(at > 0, rim[1, :, lanes].astype(jnp.float32), 0.0)
 
     stats = [
-        remote(own_stats, other_stats.at[k - 1], stat_send.at[k - 1], stat_recv.at[k - 1], "tp", lax.rem(me + k, 4))
+        remote(own_stats, other_stats.at[k - 1], stat_send.at[0], stat_recv.at[0], "tp", lax.rem(me + k, 4))
         for k in range(1, 4)
     ]
     number = len(units)
-    for u in range(0, 3):
+    def low_half(t):
+        filter_rows(pl.multiple_of(t * LANES, LANES), 1)
+
+    def high_half(t):
+        filter_rows(pl.multiple_of(t * LANES + TILE, TILE), 1)
+        tally(t)
+
+    def low_rest(t):
+        low_half(t)
+        tally(t)
+
+    whole_tiles = [far_tile + b * bigs + j for b in range(2) for j in range(1, bigs)]
+    work = []
+    for t in whole_tiles:
+        work += [functools.partial(low_half, t), functools.partial(high_half, t)]
+    work.insert(2, functools.partial(low_rest, far_tile + bigs))
+    last_work = [rim_in, functools.partial(low_rest, own_half // LANES), functools.partial(low_rest, far_tile)]
+    for _ in range(3):
+        work.pop(0)()
+    work += last_work
+    for u in range(number):
         meet(u)
-    filter_tile(far_tile + 1)
-    for u in range(3, 6):
-        meet(u)
-    filter_tile(far_tile + bigs, TILE)
-    for u in range(6, number):
-        meet(u)
-    relay(1, 0, 3)
-    if bigs > 2:
-        filter_loop(far_tile + 2, bigs - 2)
-    filter_loop(far_tile + bigs + 1, bigs - 1)
-    relay(1, 3, 6)
-    rim_in()
-    filter_tile(own_half // LANES, TILE)
-    relay(1, 6, number)
-    filter_tile(far_tile, TILE)
+        if work and u != 3:
+            work.pop(0)()
+    for one in work:
+        one()
     for one in stats:
         one.start()
+    relay(1, 0, number)
     if teams > 3:
         relay(2, 0, number)
-    for one in stats:
-        one.wait_recv()
+    all_stats = remote(other_stats, other_stats, stat_send.at[0], stat_recv.at[0], "tp", pair)
+    all_stats.wait_recv()
 
     def stats_tile(i):
         row = pl.multiple_of(i * LANES, LANES)
@@ -484,7 +505,7 @@
         lent[p].wait_recv()
         to_cross[rows, :] = (held[p % 2] + from_pair[0, rows, :].astype(jnp.float32)).astype(jnp.bfloat16)
         returned[p] = remote(
-            to_cross.at[rows, :], from_cross.at[rows, :], back_send.at[1, p], back_recv.at[1, p], "tp", cross
+            to_cross.at[rows, :], from_cross.at[rows, :], back_send.at[1], back_sem.at[p - 1], "tp", cross
         )
         returned[p].start()
 
@@ -501,7 +522,7 @@
         first_lent.append(
             remote(
                 to_pair.at[0, head_rows, cols], from_pair.at[0, head_rows, cols],
-                first_send.at[0, j], first_recv.at[0, j], "tp", pair,
+                first_send.at[0], first_recv.at[j], "tp", pair,
             )
         )
         first_lent[j].start()
@@ -514,7 +535,7 @@
         first_returned.append(
             remote(
                 to_cross.at[head_rows, cols], from_cross.at[head_rows, cols],
-                first_send.at[1, j], first_recv.at[1, j], "tp", cross,
+                first_send.at[1], first_done.at[0], "tp", cross,
             )
         )
         first_returned[j].start()
@@ -538,7 +559,7 @@
 
         spread(2 * turn, put)
         lent[p] = remote(
-            to_pair.at[0, rows, :], from_pair.at[0, rows, :], back_send.at[0, p], back_recv.at[0, p], "tp", pair
+            to_pair.at[0, rows, :], from_pair.at[0, rows, :], back_send.at[0], lent_sem.at[p - 1], "tp", pair
         )
         lent[p].start()
     settle(RETURNS - 1)
@@ -557,7 +578,7 @@
         spread(2 * CHUNK, put)
         close.append(
             remote(
-                to_pair.at[1, rows, :], from_pair.at[1, rows, :], back_send.at[2, big], back_recv.at[2, big],
+                to_pair.at[1, rows, :], from_pair.at[1, rows, :], back_send.at[2], close_sem.at[big],
                 "tp", pair,
             )
         )
@@ -566,29 +587,32 @@
         rows = pl.ds(big * CHUNK, CHUNK)
         close[big].wait_recv()
         mine[rows, :] = mine[rows, :] + from_pair[1, rows, :].astype(jnp.float32)
-    stores = []
+    first_whole = remote(
+        to_cross.at[head_rows, :], from_cross.at[head_rows, :], first_send.at[1], first_done.at[0], "tp", cross
+    )
     for p in range(RETURNS):
         rows = pl.ds(p * turn, turn)
-        for one in first_returned if p == 0 else [returned[p]]:
-            one.wait_recv()
-        done[rows, :] = (mine[rows, :] + from_cross[rows, :].astype(jnp.float32)).astype(jnp.bfloat16)
-        stores.append(pltpu.make_async_copy(done.at[rows, :], out_ref.at[rows, :], out_sem.at[p]))
-        stores[p].start()
-    for one in crossing + nearby + handed + packs + stats + first_lent + first_returned + close:
-        one.wait_send()
-    for p in range(1, RETURNS):
-        lent[p].wait_send()
-        returned[p].wait_send()
-
+        (first_whole if p == 0 else returned[p]).wait_recv()
+        out_ref[rows, :] = (mine[rows, :] + from_cross[rows, :].astype(jnp.float32)).astype(jnp.bfloat16)
+
+    def sent(ref, sem):
+        remote(ref, ref, sem, near_sem.at[0], "tp", pair).wait_send()
+
+    rest = pl.ds(turn, block - turn)
+    for k in range(3):
+        sent(near_rows.at[0], send_sem.at[k])
+    sent(pack, pack_send.at[0])
+    sent(other_stats, stat_send.at[0])
+    sent(to_pair.at[0, head_rows, :], first_send.at[0])
+    sent(to_cross.at[head_rows, :], first_send.at[1])
+    sent(to_pair.at[0, rest, :], back_send.at[0])
+    sent(to_cross.at[rest, :], back_send.at[1])
+    sent(to_pair.at[1], back_send.at[2])
     pl.when(ahead)(edge.wait_send)
 
     @pl.when(onward)
     def _():
-        for one in links:
-            one.wait_send()
-
-    for one in stores:
-        one.wait()
+        sent(chain_out, chain_send.at[0])
 
 
 def on_device(
@@ -610,8 +634,8 @@
     return pl.pallas_call(
         functools.partial(layer_kernel, head),
         in_specs=[pl.BlockSpec(memory_space=pl.ANY)] * 15,
-        out_specs=pl.BlockSpec(memory_space=pl.ANY),
-        out_shape=jax.ShapeDtypeStruct((block, columns), bf16),
+        out_specs=pl.BlockSpec(memory_space=pltpu.VMEM),
+        out_shape=pltpu.VMEM((block, columns), bf16),
         scratch_shapes=[
             vmem((1, depth), f32),
             vmem((1, width), f32),
@@ -653,27 +677,30 @@
             vmem((block, columns), bf16),
             vmem((block, columns), bf16),
             vmem((block, columns), f32),
-            vmem((block, columns), bf16),
             sems(6),
+            sems(2),
+            sems(len(weights) + 2),
+            sems(3),
             sems(SENDS),
-            sems(len(weights) + 2),
-            sems(3, SENDS),
-            sems(3, SENDS),
+            sems(1),
+            sems(block // CHUNK),
+            sems(1),
             sems(heads, 2),
-            sems(heads, 2),
-            sems(heads, 2),
+            sems(1),
             sems(heads, 2),
             sems(2),
+            sems(1),
+            sems(1),
             sems(3),
-            sems(3),
-            sems(3, RETURNS),
-            sems(3, RETURNS),
-            sems(2, columns // SPAN),
-            sems(2, columns // SPAN),
-            sems(RETURNS),
+            sems(RETURNS - 1),
+            sems(RETURNS - 1),
+            sems(block // CHUNK),
+            sems(2),
+            sems(columns // SPAN),
+            sems(1),
         ],
         compiler_params=pltpu.CompilerParams(
-            collective_id=0, has_side_effects=True, vmem_limit_bytes=65000 * 1024
+            collective_id=0, has_side_effects=True, vmem_limit_bytes=58000 * 1024
         ),
     )(
         norm_gain[None], forget_gap[None], decay_shift.T, conv_taps, conv_gain[None], head_gain[None],

time: 73 us -> 70.3 us (0.963)
  Pallas kernels: 70.6 us -> 69.2 us
  local copies, waits for them, and re-layouts: 2.3 us -> 0.97 us
    pallas_call x1, Pallas kernels: 70.6 us -> 69.2 us  [on_device(): pl.pallas_call(functools.partial(layer_kernel, head), in_specs=[pl.BlockS...]
    unnamed x1, local copies, waits for them, and re-layouts: 2.3 us -> 0.97 us
where the time goes in v4:
time: 70.3 us; the launch traced here: 70.1 us
  Pallas kernels  69.2 us (98%)
  local copies, waits for them, and re-layouts  0.97 us (1%)
    pallas_call x1, Pallas kernels, on_device(): pl.pallas_call(functools.partial(layer_kernel, head), in_specs=[pl.BlockS...  69.2 us

profile of v4, /device:TPU:25, one launch (start us, length us, event | category | flops | bytes accessed | tf_op | source)
XLA Modules:
  0.0 70.1 jit_solution(14510656284784022554)
XLA Ops:
  0.0 69.2 %shard_map.145 = bf16[256,2048]{1,0:T(8,128)(2,1)S(1)} custom-call(f32[1,2048]{1,0:T(1,128)} %bitcast.6, f32[1,512]{1,0:T(1,128)} %bitcast.7, f32[4,1024]{1,0:T(4,128)} %bitcast.5, f32[31,512]{1,0:T(8,128)} %taps_in.1, f32[1,512]{1,0:T(1,128)} %bitcast.8, f32[1,128]{1,0:T(1,128)} %bitcast.9, bf16[256,2048]{1,0:T(8,128)(2,1)} %tokens_ref.1, ...), custom_call_target="tpu_custom_call" | custom-call | tf_op jit(solution)/shard_map/pallas_call | solution.py:634
  69.2 1.0 %copy.17 = bf16[256,2048]{1,0:T(8,128)(2,1)} copy(bf16[256,2048]{1,0:T(8,128)(2,1)S(1)} %shard_map.145) | data formatting | bytes 2097152

commit v5 on v4

--- a/solution.py
+++ b/solution.py
@@ -8,7 +8,6 @@
 from jax.sharding import PartitionSpec as P
 
 CHUNK = 128
-PAD = 16
 SENDS = 8
 RETURNS = 4
 REACH = 32
@@ -39,10 +38,10 @@
     tokens_ref, w0, w1, w2, w3, w4, w5, rec_rows, conv_rows, out_ref,
     gain_ref, gap_ref, shift_ref, taps_ref, conv_gain_ref, head_gain_ref,
     raw, near_rows, far_rows, weight, merge, proj, intra, reach, local, closing, centre, enter,
-    own_state, own_log, pack, pack_in, group_state, group_log, chain_out, chain_in,
+    own_state, own_log, pack, pack_in, log_in, decay, prefix, group_state, group_log, chain_out, chain_in,
     rim, padded, filtered, own_stats, other_stats, moments,
     blend, early, held, to_pair, from_pair, to_cross, from_cross, mine,
-    small_sem, raw_sem, weight_sem, send_sem, cross_sem, near_sem, hand_sem, pack_send, pack_recv, chain_send, chain_recv,
+    small_sem, raw_sem, weight_sem, log_sem, send_sem, cross_sem, near_sem, hand_sem, pack_send, pack_recv, chain_send, chain_recv,
     rim_sem, stat_send, stat_recv, back_send, lent_sem, back_sem, close_sem, first_send, first_recv, first_done,
 ):
     block, depth = tokens_ref.shape
@@ -163,32 +162,32 @@
     def rows_of(c):
         return pl.ds(pl.multiple_of(c * CHUNK, CHUNK), CHUNK)
 
-    def state_part(several, group=None):
-        group = list(range(heads)) if group is None else group
-        wide = slice(group[0] * head, (group[-1] + 1) * head)
-        keys, totals = [], []
-        for c in several:
+    def state_part(several, ready=None):
+        keys, totals, values = [], [], []
+        for k, c in enumerate(several):
             rows = rows_of(c)
-            key = gap_ref[:, wide] * jax.nn.sigmoid(-proj[FORGET, rows, wide].astype(jnp.float32))
-            shift = [jnp.broadcast_to(shift_ref[h : h + 1, rows], (head, CHUNK)).T for h in group]
+            forget = proj[FORGET, rows, :] if ready is None else ready[0][k * CHUNK : (k + 1) * CHUNK]
+            values.append(proj[VALUE, rows, :] if ready is None else ready[1][k * CHUNK : (k + 1) * CHUNK])
+            key = gap_ref[...] * jax.nn.sigmoid(-forget.astype(jnp.float32))
+            shift = [jnp.broadcast_to(shift_ref[h : h + 1, rows], (head, CHUNK)).T for h in range(heads)]
             log = jnp.log1p(-key) + jnp.concatenate(shift, axis=1)
             high = log.astype(jnp.bfloat16)
             low = (log - high.astype(jnp.float32)).astype(jnp.bfloat16)
             keys.append(key)
             totals.append(dot(lower, jnp.concatenate([high, low], axis=0)))
-        for c, key, total in zip(several, keys, totals):
+        for c, key, total, value in zip(several, keys, totals, values):
             rows = rows_of(c)
             last = total[CHUNK - 1 : CHUNK, :]
             middle = total[CHUNK // 2 - 1 : CHUNK // 2, :]
             total = total - middle
             key_mid = key * jnp.exp(-total)
-            intra[rows, wide] = total
-            reach[rows, wide] = key_mid.astype(jnp.bfloat16)
+            intra[rows, :] = total
+            reach[rows, :] = key_mid.astype(jnp.bfloat16)
             key_end = (key_mid * jnp.exp(last - middle)).astype(jnp.bfloat16)
-            for i, h in enumerate(group):
-                local[c, h] = dot(proj[VALUE, rows, parts[h]], key_end[:, parts[i]], ((0,), (0,)))
-            closing[c, :, wide] = last
-            centre[c, :, wide] = middle
+            for h, part in enumerate(parts):
+                local[c, h] = dot(value[:, part], key_end[:, part], ((0,), (0,)))
+            closing[c] = last
+            centre[c] = middle
 
     def query_part(several):
         queries, scores = [], []
@@ -305,37 +304,41 @@
         for p in range(begin + 2 * per - 2, begin + 2 * per):
             pass_on(p)
     handed_in(bigs - 1)
-    project(far_rows.at[bigs - 1], 0, 2, far_places(bigs - 1))
-
-    place = lax.broadcasted_iota(jnp.int32, (PAD, head), 0)
+
     half = head // 2
     units = [(h, k) for h in range(heads) for k in range(2)]
-    spans = (pl.ds(0, PAD + half), pl.ds(PAD + half, half))
+    spans = (pl.ds(0, half), pl.ds(half, half))
     packs = [
         remote(pack.at[h, spans[k], :], pack_in.at[h, spans[k], :], pack_send.at[0], pack_recv.at[h, k], "sp", mate)
         for h, k in units
     ]
     def send_state(h):
-        part = slice(h * head, (h + 1) * head)
-        state, log = local[0, h], closing[0, :, part]
+        state = local[0, h]
+        prefix[0, h] = jnp.zeros_like(state)
         for c in range(1, chunks):
-            state = state * jnp.exp(closing[c, :, part]) + local[c, h]
-            log = log + closing[c, :, part]
+            prefix[c, h] = state
+            state = state * jnp.exp(closing[c, :, parts[h]]) + local[c, h]
         own_state[h] = state
-        own_log[:, part] = log
-        pack[h, PAD : PAD + head, :] = state.astype(jnp.bfloat16)
-        high = log.astype(jnp.bfloat16).astype(jnp.float32)
-        rest = log - high
-        mid = rest.astype(jnp.bfloat16).astype(jnp.float32)
-        low = rest - mid
-        tail = jnp.where(place == 0, high, jnp.where(place == 1, mid, jnp.where(place == 2, low, 0.0)))
-        pack[h, 0:PAD, :] = tail.astype(jnp.bfloat16)
+        pack[h] = state.astype(jnp.bfloat16)
         packs[2 * h].start()
         packs[2 * h + 1].start()
 
-    state_part(far_chunks(bigs - 1))
+    gates, inputs = [dot(far_rows[bigs - 1], weight[i]).astype(jnp.bfloat16) for i in (FORGET, VALUE)]
+    for start, row, size in far_places(bigs - 1):
+        proj[VALUE, pl.ds(pl.multiple_of(row, CHUNK), size), :] = inputs[start : start + size]
+    state_part(far_chunks(bigs - 1), (gates, inputs))
+    log = closing[0]
+    for c in range(1, chunks):
+        log = log + closing[c]
+    own_log[...] = log
+    logs = remote(own_log, log_in, log_sem.at[0], log_sem.at[1], "sp", mate)
+    logs.start()
     for h in range(heads):
         send_state(h)
+    log = jnp.zeros_like(log)
+    for c in range(chunks):
+        decay[c] = jnp.exp(log)
+        log = log + closing[c]
     project(far_rows.at[bigs - 1], 2, 4, far_places(bigs - 1))
     for _, row, size in far_places(bigs - 1):
         mix(row, size)
@@ -354,14 +357,15 @@
     ]
 
     def mate_log(h):
-        tail = pack_in[h, 0:PAD, :].astype(jnp.float32)
-        return tail[0:1] + tail[1:2] + tail[2:3]
+        return log_in[:, parts[h]]
 
     def meet(u):
         h, k = units[u]
         some = pl.ds(k * half, half)
+        if u == 0:
+            logs.wait_recv()
         packs[u].wait_recv()
-        theirs, log = pack_in[h, PAD + k * half : PAD + (k + 1) * half, :].astype(jnp.float32), mate_log(h)
+        theirs, log = pack_in[h, some, :].astype(jnp.float32), mate_log(h)
         ours, own = own_state[h, some, :], own_log[:, parts[h]]
         first = jnp.where(side == 0, ours, theirs)
         second = jnp.where(side == 0, theirs, ours)
@@ -421,11 +425,13 @@
         meet(u)
         if work and u != 3:
             work.pop(0)()
+        if u >= 5:
+            relay(1, u - 5, u - 4)
     for one in work:
         one()
     for one in stats:
         one.start()
-    relay(1, 0, number)
+    relay(1, number - 5, number)
     if teams > 3:
         relay(2, 0, number)
     all_stats = remote(other_stats, other_stats, stat_send.at[0], stat_recv.at[0], "tp", pair)
@@ -476,14 +482,16 @@
         relay(k, 0, number)
 
     for h in range(heads):
-        part = slice(h * head, (h + 1) * head)
         state = chain_in[h].astype(jnp.float32)
-        moved = state * jnp.exp(mate_log(h)) + pack_in[h, PAD : PAD + head, :].astype(jnp.float32)
-        state = jnp.where(side == 1, moved, state)
-        for c in range(chunks):
-            enter[c, h] = state.astype(jnp.bfloat16)
-            if c < chunks - 1:
-                state = state * jnp.exp(closing[c, :, part]) + local[c, h]
+        moved = state * jnp.exp(mate_log(h)) + pack_in[h].astype(jnp.float32)
+        own_state[h] = jnp.where(side == 1, moved, state)
+
+    def enter_chunk(c):
+        for h in range(heads):
+            enter[c, h] = (own_state[h] * decay[c, :, parts[h]] + prefix[c, h]).astype(jnp.bfloat16)
+
+    for owner in (diag, cross):
+        enter_chunk(owner * bigs)
 
     def rec_part(owner, low, size, slot):
         rows, target = pl.ds(pl.multiple_of(owner * block + low, size), size), pl.ds(slot, size)
@@ -548,6 +556,7 @@
             for owner in (diag, cross):
                 for big in range(1, bigs):
                     stats_tile(owner * bigs + big)
+                    enter_chunk(owner * bigs + big)
         finish_rows(diag, p * turn, turn, 0)
         finish_rows(cross, p * turn, turn, turn)
         if p > 1 and p != late:
@@ -566,6 +575,7 @@
     for owner in (pair, me):
         for big in range(bigs):
             stats_tile(owner * bigs + big)
+            enter_chunk(owner * bigs + big)
     for big in range(bigs):
         rows = pl.ds(big * CHUNK, CHUNK)
         finish_rows(pair, big * CHUNK, CHUNK, 0)
@@ -602,6 +612,7 @@
     for k in range(3):
         sent(near_rows.at[0], send_sem.at[k])
     sent(pack, pack_send.at[0])
+    logs.wait_send()
     sent(other_stats, stat_send.at[0])
     sent(to_pair.at[0, head_rows, :], first_send.at[0])
     sent(to_cross.at[head_rows, :], first_send.at[1])
@@ -657,8 +668,11 @@
             vmem((chunks, heads, head, head), bf16),
             vmem((heads, head, head), f32),
             vmem((1, width), f32),
-            vmem((heads, head + PAD, head), bf16),
-            vmem((heads, head + PAD, head), bf16),
+            vmem((heads, head, head), bf16),
+            vmem((heads, head, head), bf16),
+            vmem((1, width), f32),
+            vmem((chunks, 1, width), f32),
+            vmem((chunks, heads, head, head), f32),
             vmem((heads, head, head), f32),
             vmem((1, width), f32),
             vmem((heads, head, head), bf16),
@@ -680,6 +694,7 @@
             sems(6),
             sems(2),
             sems(len(weights) + 2),
+            sems(2),
             sems(3),
             sems(SENDS),
             sems(1),

time: 70.3 us -> 69.2 us (0.984)
  Pallas kernels: 69.2 us -> 67.9 us
    pallas_call x1, Pallas kernels: 69.2 us -> 67.9 us  [on_device(): pl.pallas_call(functools.partial(layer_kernel, head), in_specs=[pl.BlockS...]
where the time goes in v5:
time: 69.2 us; the launch traced here: 68.9 us
  Pallas kernels  67.9 us (98%)
  local copies, waits for them, and re-layouts  0.97 us (1%)
    pallas_call x1, Pallas kernels, on_device(): pl.pallas_call(functools.partial(layer_kernel, head), in_specs=[pl.BlockS...  67.9 us

profile of v5, /device:TPU:25, one launch (start us, length us, event | category | flops | bytes accessed | tf_op | source)
XLA Modules:
  0.0 68.9 jit_solution(8010117977615721342)
XLA Ops:
  0.0 67.9 %shard_map.145 = bf16[256,2048]{1,0:T(8,128)(2,1)S(1)} custom-call(f32[1,2048]{1,0:T(1,128)} %bitcast.6, f32[1,512]{1,0:T(1,128)} %bitcast.7, f32[4,1024]{1,0:T(4,128)} %bitcast.5, f32[31,512]{1,0:T(8,128)} %taps_in.1, f32[1,512]{1,0:T(1,128)} %bitcast.8, f32[1,128]{1,0:T(1,128)} %bitcast.9, bf16[256,2048]{1,0:T(8,128)(2,1)} %tokens_ref.1, ...), custom_call_target="tpu_custom_call" | custom-call | tf_op jit(solution)/shard_map/pallas_call | solution.py:645
  67.9 1.0 %copy.17 = bf16[256,2048]{1,0:T(8,128)(2,1)} copy(bf16[256,2048]{1,0:T(8,128)(2,1)S(1)} %shard_map.145) | data formatting | bytes 2097152

commit v6 on v5

--- a/solution.py
+++ b/solution.py
@@ -14,6 +14,7 @@
 TILE = 64
 LANES = 128
 SPAN = 512
+STRAIGHT = 256
 MESH = pl.DeviceIdType.MESH
 FORGET, VALUE, GLU_VALUE, GLU_GATE, QUERY, RGATE = range(6)
 
@@ -40,9 +41,9 @@
     raw, near_rows, far_rows, weight, merge, proj, intra, reach, local, closing, centre, enter,
     own_state, own_log, pack, pack_in, log_in, decay, prefix, group_state, group_log, chain_out, chain_in,
     rim, padded, filtered, own_stats, other_stats, moments,
-    blend, early, held, to_pair, from_pair, to_cross, from_cross, mine,
+    blend, early, straight_out, straight_in, held, to_pair, from_pair, to_cross, from_cross, mine,
     small_sem, raw_sem, weight_sem, log_sem, send_sem, cross_sem, near_sem, hand_sem, pack_send, pack_recv, chain_send, chain_recv,
-    rim_sem, stat_send, stat_recv, back_send, lent_sem, back_sem, close_sem, first_send, first_recv, first_done,
+    rim_sem, stat_send, stat_recv, back_send, lent_sem, back_sem, close_sem, first_send, first_recv, first_done, straight_sem,
 ):
     block, depth = tokens_ref.shape
     piece = block // SENDS
@@ -522,9 +523,20 @@
     first_lent, first_returned = [], []
     rec_part(diag, 0, turn, 0)
     rec_part(cross, 0, turn, turn)
-    for j in range(columns // SPAN):
-        cols = slice(j * SPAN, (j + 1) * SPAN)
-        result = dot(blend[0 : 2 * turn, 0:width], merge[0:width, cols]) + early[:, cols]
+    straight = [
+        remote(straight_out.at[k], straight_in.at[k], straight_sem.at[0], straight_sem.at[1], "tp", device)
+        for k, device in enumerate((cross, diag))
+    ]
+    splits = [slice(max(j * SPAN, STRAIGHT), (j + 1) * SPAN) for j in range(columns // SPAN)]
+    for j, cols in enumerate(splits):
+        wide = slice(j * SPAN, (j + 1) * SPAN)
+        result = dot(blend[0 : 2 * turn, 0:width], merge[0:width, wide]) + early[:, wide]
+        if j == 0:
+            straight_out[0] = result[turn : 2 * turn, 0:STRAIGHT].astype(jnp.bfloat16)
+            straight_out[1] = result[0:turn, 0:STRAIGHT].astype(jnp.bfloat16)
+            for one in straight:
+                one.start()
+            result = result[:, STRAIGHT:]
         to_pair[0, head_rows, cols] = result[0:turn].astype(jnp.bfloat16)
         held[0, :, cols] = result[turn : 2 * turn]
         first_lent.append(
@@ -534,8 +546,7 @@
             )
         )
         first_lent[j].start()
-    for j in range(columns // SPAN):
-        cols = slice(j * SPAN, (j + 1) * SPAN)
+    for j, cols in enumerate(splits):
         first_lent[j].wait_recv()
         to_cross[head_rows, cols] = (held[0, :, cols] + from_pair[0, head_rows, cols].astype(jnp.float32)).astype(
             jnp.bfloat16
@@ -597,13 +608,19 @@
         rows = pl.ds(big * CHUNK, CHUNK)
         close[big].wait_recv()
         mine[rows, :] = mine[rows, :] + from_pair[1, rows, :].astype(jnp.float32)
+    summed = pl.ds(STRAIGHT, columns - STRAIGHT)
     first_whole = remote(
-        to_cross.at[head_rows, :], from_cross.at[head_rows, :], first_send.at[1], first_done.at[0], "tp", cross
+        to_cross.at[head_rows, summed], from_cross.at[head_rows, summed], first_send.at[1], first_done.at[0],
+        "tp", cross,
     )
+    remote(straight_in, straight_in, straight_sem.at[0], straight_sem.at[1], "tp", cross).wait_recv()
+    across = straight_in[0].astype(jnp.float32) + straight_in[1].astype(jnp.float32)
+    out_ref[head_rows, 0:STRAIGHT] = (mine[head_rows, 0:STRAIGHT] + across).astype(jnp.bfloat16)
     for p in range(RETURNS):
         rows = pl.ds(p * turn, turn)
         (first_whole if p == 0 else returned[p]).wait_recv()
-        out_ref[rows, :] = (mine[rows, :] + from_cross[rows, :].astype(jnp.float32)).astype(jnp.bfloat16)
+        cols = summed if p == 0 else pl.ds(0, columns)
+        out_ref[rows, cols] = (mine[rows, cols] + from_cross[rows, cols].astype(jnp.float32)).astype(jnp.bfloat16)
 
     def sent(ref, sem):
         remote(ref, ref, sem, near_sem.at[0], "tp", pair).wait_send()
@@ -614,8 +631,9 @@
     sent(pack, pack_send.at[0])
     logs.wait_send()
     sent(other_stats, stat_send.at[0])
-    sent(to_pair.at[0, head_rows, :], first_send.at[0])
-    sent(to_cross.at[head_rows, :], first_send.at[1])
+    sent(to_pair.at[0, head_rows, summed], first_send.at[0])
+    sent(to_cross.at[head_rows, summed], first_send.at[1])
+    sent(straight_in, straight_sem.at[0])
     sent(to_pair.at[0, rest, :], back_send.at[0])
     sent(to_cross.at[rest, :], back_send.at[1])
     sent(to_pair.at[1], back_send.at[2])
@@ -685,6 +703,8 @@
             vmem((2, rows, LANES), f32),
             vmem((2 * CHUNK, 2 * width), bf16),
             vmem((2 * turn, columns), f32),
+            vmem((2, turn, STRAIGHT), bf16),
+            vmem((2, turn, STRAIGHT), bf16),
             vmem((2, turn, columns), f32),
             vmem((2, block, columns), bf16),
             vmem((2, block, columns), bf16),
@@ -713,6 +733,7 @@
             sems(2),
             sems(columns // SPAN),
             sems(1),
+            sems(2),
         ],
         compiler_params=pltpu.CompilerParams(
             collective_id=0, has_side_effects=True, vmem_limit_bytes=58000 * 1024

time: 69.2 us -> 68.6 us (level)
  no operation moved by 1% of the time
where the time goes in v6:
time: 68.6 us; the launch traced here: 68.4 us
  Pallas kernels  67.4 us (98%)
  local copies, waits for them, and re-layouts  0.97 us (1%)
    pallas_call x1, Pallas kernels, on_device(): pl.pallas_call(functools.partial(layer_kernel, head), in_specs=[pl.BlockS...  67.4 us

profile of v6, /device:TPU:25, one launch (start us, length us, event | category | flops | bytes accessed | tf_op | source)
XLA Modules:
  0.0 68.4 jit_solution(4407965237681430188)
XLA Ops:
  0.0 67.4 %shard_map.145 = bf16[256,2048]{1,0:T(8,128)(2,1)S(1)} custom-call(f32[1,2048]{1,0:T(1,128)} %bitcast.6, f32[1,512]{1,0:T(1,128)} %bitcast.7, f32[4,1024]{1,0:T(4,128)} %bitcast.5, f32[31,512]{1,0:T(8,128)} %taps_in.1, f32[1,512]{1,0:T(1,128)} %bitcast.8, f32[1,128]{1,0:T(1,128)} %bitcast.9, bf16[256,2048]{1,0:T(8,128)(2,1)} %tokens_ref.1, ...), custom_call_target="tpu_custom_call" | custom-call | tf_op jit(solution)/shard_map/pallas_call | solution.py:663
  67.4 1.0 %copy.17 = bf16[256,2048]{1,0:T(8,128)(2,1)} copy(bf16[256,2048]{1,0:T(8,128)(2,1)S(1)} %shard_map.145) | data formatting | bytes 2097152

commit v7 on v6

--- a/solution.py
+++ b/solution.py
@@ -85,7 +85,6 @@
         pl.semaphore_signal(barrier, inc=1, device_id={"sp": at - 1}, device_id_type=MESH)
 
     onward = team < teams - 1
-    pl.semaphore_wait(barrier, jnp.where(onward, jnp.where(side == 1, 6, 5), 4))
 
     rows_all = proj.shape[1]
     heads, chunks = width // head, rows_all // CHUNK
@@ -100,10 +99,8 @@
             device_id={axis: device}, device_id_type=MESH,
         )
 
-    smalls[0].wait()
-
-    crossing, nearby, handed = [], [], []
-    for p in range(SENDS):
+
+    def norm_rows(p):
         rows = pl.ds(p * piece, piece)
         if p < 2:
             raws[p].wait()
@@ -111,6 +108,16 @@
             for one in fetched:
                 one.start()
         near_rows[0, rows, :] = layer_norm(raw[rows, :], gain_ref[...]).astype(jnp.bfloat16)
+
+    smalls[0].wait()
+    norm_rows(0)
+    pl.semaphore_wait(barrier, jnp.where(onward, jnp.where(side == 1, 6, 5), 4))
+
+    crossing, nearby, handed = [], [], []
+    for p in range(SENDS):
+        rows = pl.ds(p * piece, piece)
+        if p > 0:
+            norm_rows(p)
         big, low = p // per, (p % per) * piece
         landing = far_rows.at[big, pl.ds(low, piece), :]
         crossing.append(remote(near_rows.at[0, rows, :], landing, send_sem.at[0], cross_sem.at[p], "tp", cross))
@@ -125,7 +132,10 @@
                 send_sem.at[2], hand_sem.at[big], "tp", pair,
             )
         )
-        crossing[p].start()
+        if p < SENDS - 1:
+            crossing[p].start()
+        else:
+            pl.when(lax.rem(me, 2) == 0)(crossing[p].start)
         nearby[p].start()
     for one in smalls[1:]:
         one.wait()
@@ -299,6 +309,7 @@
         for p in range(begin + per + 1, begin + 2 * per - 2):
             pass_on(p)
         if big == bigs - 2:
+            pl.when(lax.rem(me, 2) == 1)(crossing[SENDS - 1].start)
             filter_tile(own_half // LANES + half_tiles - 1)
             for tile in (own_half // LANES, far_tile, far_tile + bigs):
                 filter_rows(pl.multiple_of(tile * LANES + TILE, TILE), 1)

time: 68.6 us -> 68.2 us (level)
  no operation moved by 1% of the time
where the time goes in v7:
time: 68.2 us; the launch traced here: 67.8 us
  Pallas kernels  66.8 us (98%)
  local copies, waits for them, and re-layouts  0.97 us (1%)
    pallas_call x1, Pallas kernels, on_device(): pl.pallas_call(functools.partial(layer_kernel, head), in_specs=[pl.BlockS...  66.8 us

profile of v7, /device:TPU:25, one launch (start us, length us, event | category | flops | bytes accessed | tf_op | source)
XLA Modules:
  0.0 67.8 jit_solution(6761887155918675209)
XLA Ops:
  0.0 66.8 %shard_map.145 = bf16[256,2048]{1,0:T(8,128)(2,1)S(1)} custom-call(f32[1,2048]{1,0:T(1,128)} %bitcast.6, f32[1,512]{1,0:T(1,128)} %bitcast.7, f32[4,1024]{1,0:T(4,128)} %bitcast.5, f32[31,512]{1,0:T(8,128)} %taps_in.1, f32[1,512]{1,0:T(1,128)} %bitcast.8, f32[1,128]{1,0:T(1,128)} %bitcast.9, bf16[256,2048]{1,0:T(8,128)(2,1)} %tokens_ref.1, ...), custom_call_target="tpu_custom_call" | custom-call | tf_op jit(solution)/shard_map/pallas_call | solution.py:674
  66.8 1.0 %copy.17 = bf16[256,2048]{1,0:T(8,128)(2,1)} copy(bf16[256,2048]{1,0:T(8,128)(2,1)S(1)} %shard_map.145) | data formatting | bytes 2097152
